TPU v7x, 128 devices: a whole 4x4x4 slice. The times are simulated.
128 devices in a mesh: sp: 32 (over z, y, core), tp: 4 (over x).
Axes of the slice: x: 4, y: 4, z: 4, core: 2. Of those that a mesh axis runs over, the one named last changes fastest.
Arguments:
- mixer_value_projection: bfloat16 [24576, 2048], P('sp', 'tp'), may hold values from -6 to 6
- write_vectors_projected: bfloat16 [24576, 256], P('sp', 'tp'), may hold values from -6 to 6
- read_vectors_projected: bfloat16 [24576, 256], P('sp', 'tp'), may hold values from -6 to 6
- output_gate_projected: bfloat16 [24576, 2048], P('sp', 'tp'), may hold values from -6 to 6
- step_size_scores: float32 [24576, 32], P('sp', 'tp'), may hold values from -8 to 8
- position_decay_extra: float32 [24576, 32], P('sp', 'tp'), may hold values from -1 to 0
- step_size_bias: float32 [32], P('tp'), may hold values from -1 to 1
- head_decay_logarithm: float32 [32], P('tp'), may hold values from -14 to -3
- value_filter_taps: bfloat16 [4, 2048], P(None, 'tp'), may hold values from -3 to 3
- write_filter_taps: bfloat16 [4, 256], P(None, 'tp'), may hold values from -3 to 3
- read_filter_taps: bfloat16 [4, 256], P(None, 'tp'), may hold values from -3 to 3
- gated_group_norm_gain: float32 [2048], P('tp'), may hold values from 0.1 to 1.9
- mixer_output_weight: bfloat16 [2048, 2048], P('tp'), may hold values from -0.125 to 0.125
- residual: bfloat16 [24576, 2048], P('sp'), may hold values from -6 to 6
- feedforward_norm_gain: float32 [2048], replicated, may hold values from 0.1 to 1.9
- feedforward_gate_weight: bfloat16 [2048, 5632], P('sp', 'tp'), may hold values from -0.125 to 0.125
- feedforward_value_weight: bfloat16 [2048, 5632], P('sp', 'tp'), may hold values from -0.125 to 0.125
- gate_filter_taps: bfloat16 [3, 5632], P(None, 'tp'), may hold values from -3.5 to 3.5
- single_value_filter_taps: bfloat16 [3, 5632], P(None, 'tp'), may hold values from -3.5 to 3.5
- feedforward_down_weight: bfloat16 [5632, 2048], P('tp', 'sp'), may hold values from -0.078125 to 0.078125
Outputs:
- mixed: bfloat16 [24576, 2048], P(('sp', 'tp'))
All inputs are finite; a program needn't handle non-finite values.
Results may differ from a plain program's by a relative error of at most 0.012.
Values may be sent and summed in bfloat16 or wider, within the bound.
No kernel may reach another device: no remote copies, remote signals or barrier semaphores. Data moves between devices by JAX's collectives and lax.ppermute only.
A program may use at most 192 MiB of HBM per device.

v0:
```python
import jax
import jax.numpy as jnp
from jax import lax
from jax.experimental import pallas as pl
from jax.experimental.pallas import tpu as pltpu
from jax.sharding import Mesh
from jax.sharding import PartitionSpec as P


HEAD = 64
STATE = 64
BLOCK = 128
RIM = 16
SP = ("sp_0", "sp_1", "sp_2")
SP_TP = ("sp_0", "sp_1", "sp_2", "tp")
BF = jnp.bfloat16
F32 = jnp.float32

epsilon = 1e-06


def shifted(value, axis, by, wrap=False):
    length = lax.axis_size(axis)
    if wrap:
        pairs = [(i, (i + by) % length) for i in range(length)]
    else:
        pairs = [(i, i + by) for i in range(length) if 0 <= i + by < length]
    return lax.ppermute(value, axis, pairs)


def swapped(value):
    return lax.ppermute(value, "sp_2", [(0, 1), (1, 0)])


def turned(value, phase, by):
    zs, ys, cs = (lax.axis_size(axis) for axis in SP)
    pairs = []
    for z in range(zs):
        for y in range(ys):
            for c in range(cs):
                to_z, to_y = (z, (y + by) % ys) if c == phase else ((z + by) % zs, y)
                pairs.append(((z * ys + y) * cs + c, (to_z * ys + to_y) * cs + c))
    return lax.ppermute(value, SP, pairs)


def short_ring(step, value):
    behind = step(value, 1)
    ahead = step(value, -1)
    far = step(behind, 1)
    return behind, ahead, far


def named_swaps(values):
    result = []
    for value in values:
        result.append(swapped(value))
    return result


def sent_to_all(value, axis):
    length = lax.axis_size(axis)
    return lax.all_to_all(
        jnp.broadcast_to(value[None], (length, *value.shape)), axis, 0, 0, tiled=True
    )


def silu(v):
    return v / (1.0 + jnp.exp(-v))


def rolled_taps(before, current, taps):
    count = taps.shape[0]
    rows = current.shape[0]
    padded = jnp.concatenate([before, current], 0)
    result = taps[count - 1 : count].astype(F32) * current
    for back in range(1, count):
        moved = pltpu.roll(padded, back, 0)[8 : 8 + rows]
        result = result + taps[count - 1 - back : count - back].astype(F32) * moved
    return result


def halves(a, axis):
    high = a.astype(BF)
    return jnp.concatenate([high, (a - high.astype(F32)).astype(BF)], axis)


def thirds(a, axis):
    high = a.astype(BF)
    rest = a - high.astype(F32)
    middle = rest.astype(BF)
    return jnp.concatenate([high, middle, (rest - middle.astype(F32)).astype(BF)], axis)


def head_lanes(heads, inner):
    one = (
        lax.broadcasted_iota(jnp.int32, (heads, inner), 1) // HEAD
        == lax.broadcasted_iota(jnp.int32, (heads, inner), 0)
    ).astype(F32)
    return jnp.concatenate([one, one], 0).astype(BF)


def spread(by_head, lanes):
    return lax.dot_general(
        halves(by_head, 0), lanes, (((0,), (0,)), ((), ())), preferred_element_type=F32
    )


def mixer_kernel(
    x_ref, w_ref, r_ref, rim_ref, dt_ref, ex_ref, bias_ref, rate_ref,
    tx_ref, tw_ref, tr_ref,
    scaled_ref, write_ref, read_ref, before_ref, cum_ref, grow_ref, state_ref,
    carry, total, bx, bw, br,
):
    step_index = pl.program_id(0)
    heads = dt_ref.shape[0]
    size, inner = x_ref.shape

    @pl.when(step_index == 0)
    def _():
        carry[...] = jnp.zeros_like(carry)
        total[...] = jnp.zeros_like(total)
        rim = rim_ref[RIM - 8 :, : inner + 2 * STATE].astype(F32)
        bx[...] = rim[:, :inner]
        bw[...] = rim[:, inner : inner + STATE]
        br[...] = rim[:, inner + STATE :]

    cx = x_ref[...].astype(F32)
    cw = w_ref[...].astype(F32).T
    cr = r_ref[...].astype(F32).T
    x = silu(rolled_taps(bx[...], cx, tx_ref[...])).astype(BF)
    write = silu(rolled_taps(bw[...], cw, tw_ref[...])).astype(BF)
    read = silu(rolled_taps(br[...], cr, tr_ref[...])).astype(BF)
    bx[...] = cx[size - 8 :]
    bw[...] = cw[size - 8 :]
    br[...] = cr[size - 8 :]
    write_ref[...] = write
    read_ref[...] = read

    lanes = head_lanes(heads, inner)
    column = lambda a: jnp.broadcast_to(a, (heads, heads)).T[:, :1]
    raw = dt_ref[...] + column(bias_ref[...])
    step = jnp.maximum(raw, 0.0) + jnp.log1p(jnp.exp(-jnp.abs(raw)))
    log_decay = -step * jnp.exp(column(rate_ref[...])) + ex_ref[...]
    upper = (
        lax.broadcasted_iota(jnp.int32, (BLOCK, BLOCK), 0)
        <= lax.broadcasted_iota(jnp.int32, (BLOCK, BLOCK), 1)
    ).astype(F32).astype(BF)
    state = carry[...]
    sum_before = total[...]
    scaled = (x.astype(F32) * spread(step, lanes)).astype(BF)
    scaled_ref[...] = scaled
    for k in range(size // BLOCK):
        here = slice(k * BLOCK, (k + 1) * BLOCK)
        parts = jnp.dot(thirds(log_decay[:, here], 0), upper, preferred_element_type=F32)
        cum = parts[:heads] + parts[heads : 2 * heads] + parts[2 * heads :]
        end = cum[:, BLOCK - 1 :]
        cum_ref[:, here] = cum
        grow_ref[:, here] = jnp.exp(cum + sum_before[:, :1])
        before_ref[k * STATE : (k + 1) * STATE, :] = state
        tails = spread(jnp.exp(end - cum), lanes)
        tailed = (scaled[here].astype(F32) * tails).astype(BF)
        fresh = lax.dot_general(
            write[here], tailed, (((0,), (0,)), ((), ())), preferred_element_type=F32
        )
        decay = spread(jnp.broadcast_to(jnp.exp(end), (heads, BLOCK)), lanes)
        state = state * decay[:1] + fresh
        sum_before = sum_before + end
    carry[...] = state
    total[...] = sum_before

    @pl.when(step_index == pl.num_programs(0) - 1)
    def _():
        state_ref[:STATE, :] = state.astype(BF)
        decay = spread(jnp.exp(sum_before), lanes)
        state_ref[STATE:, :] = decay[:RIM].astype(BF)


def mixer_local(x, w, r, rim, dt, ex, bias, rate, tx, tw, tr):
    rows, inner = x.shape
    heads = dt.shape[0]
    size = 2 * BLOCK
    by_block = lambda width: pl.BlockSpec((size, width), lambda b: (b, 0))
    by_lanes = pl.BlockSpec((heads, size), lambda b: (0, b))
    by_channel = pl.BlockSpec((STATE, size), lambda b: (0, b))
    whole = lambda a: pl.BlockSpec(a.shape, lambda b: (0, 0))
    shape = jax.ShapeDtypeStruct
    blocks = rows // BLOCK
    return pl.pallas_call(
        mixer_kernel,
        grid=(rows // size,),
        in_specs=[by_block(inner), by_channel, by_channel, whole(rim), by_lanes, by_lanes]
        + [whole(a) for a in (bias, rate, tx, tw, tr)],
        out_specs=[
            by_block(inner),
            by_block(STATE),
            by_block(STATE),
            pl.BlockSpec((size // BLOCK * STATE, inner), lambda b: (b, 0)),
            by_lanes,
            by_lanes,
            pl.BlockSpec((STATE + RIM, inner), lambda b: (0, 0)),
        ],
        out_shape=[
            shape((rows, inner), BF),
            shape((rows, STATE), BF),
            shape((rows, STATE), BF),
            shape((blocks * STATE, inner), F32),
            shape((heads, rows), F32),
            shape((heads, rows), F32),
            shape((STATE + RIM, inner), BF),
        ],
        scratch_shapes=[
            pltpu.VMEM((STATE, inner), F32),
            pltpu.VMEM((heads, BLOCK), F32),
            pltpu.VMEM((8, inner), F32),
            pltpu.VMEM((8, STATE), F32),
            pltpu.VMEM((8, STATE), F32),
        ],
        name="mixer_local",
    )(x, w, r, rim, dt, ex, bias, rate, tx, tw, tr)


def entered(read, state):
    return jnp.dot(
        jnp.concatenate([read, read], 1), halves(state, 0), preferred_element_type=F32
    )


def inside_kernel(scaled_ref, write_ref, read_ref, before_ref, cum_ref, y_ref):
    heads = cum_ref.shape[0]
    size, inner = scaled_ref.shape
    lanes = head_lanes(heads, inner)
    rows = lax.broadcasted_iota(jnp.int32, (BLOCK, BLOCK), 0)
    cols = lax.broadcasted_iota(jnp.int32, (BLOCK, BLOCK), 1)
    causal = rows >= cols
    first_half = lax.broadcasted_iota(jnp.int32, (BLOCK, 2 * HEAD), 1) < HEAD
    for k in range(size // BLOCK):
        here = slice(k * BLOCK, (k + 1) * BLOCK)
        read = read_ref[here, :]
        scaled = scaled_ref[here, :]
        cum_t = cum_ref[:, here]
        cum = cum_t.T
        scores = lax.dot_general(
            read, write_ref[here, :], (((1,), (1,)), ((), ())), preferred_element_type=F32
        )
        pieces = []
        for pair in range(heads // 2):
            values = scaled[:, pair * 2 * HEAD : (pair + 1) * 2 * HEAD]
            both = []
            for h in (2 * pair, 2 * pair + 1):
                gap = cum[:, h : h + 1] - cum_t[h : h + 1, :]
                both.append((scores * jnp.exp(jnp.where(causal, gap, -1e30))).astype(BF))
            product = jnp.dot(jnp.concatenate(both, 0), values, preferred_element_type=F32)
            pieces.append(jnp.where(first_half, product[:BLOCK], product[BLOCK:]))
        before = before_ref[k * STATE : (k + 1) * STATE, :]
        grown = spread(jnp.exp(cum_t), lanes)
        y_ref[here, :] = jnp.concatenate(pieces, 1) + grown * entered(read, before)


def mixer_inside(scaled, write, read, before, cum):
    rows, inner = scaled.shape
    heads = cum.shape[0]
    size = 2 * BLOCK
    by_block = lambda width: pl.BlockSpec((size, width), lambda b: (b, 0))
    return pl.pallas_call(
        inside_kernel,
        grid=(rows // size,),
        in_specs=[
            by_block(inner),
            by_block(STATE),
            by_block(STATE),
            pl.BlockSpec((size // BLOCK * STATE, inner), lambda b: (b, 0)),
            pl.BlockSpec((heads, size), lambda b: (0, b)),
        ],
        out_specs=by_block(inner),
        out_shape=jax.ShapeDtypeStruct((rows, inner), F32),
        name="mixer_inside",
    )(scaled, write, read, before, cum)


def finish_kernel(y_ref, read_ref, grow_ref, gate_ref, state_ref, gain_ref, top_ref, low_ref):
    grown = spread(grow_ref[...], head_lanes(grow_ref.shape[0], y_ref.shape[1]))
    mixer = y_ref[...] + grown * entered(read_ref[...], state_ref[...])
    gated = mixer * silu(gate_ref[...].astype(F32))
    mean = jnp.mean(gated * gated, axis=-1, keepdims=True)
    normed = (gated * lax.rsqrt(mean + epsilon) * gain_ref[...]).astype(BF)

    @pl.when(pl.program_id(0) == 0)
    def _():
        top_ref[...] = normed

    @pl.when(pl.program_id(0) == 1)
    def _():
        low_ref[...] = normed


def mixer_finish(y, read, grow, gate, state, gain):
    rows, inner = y.shape
    heads = grow.shape[0]
    size = rows // 2
    by_block = lambda width: pl.BlockSpec((size, width), lambda b: (b, 0))
    whole = lambda a: pl.BlockSpec(a.shape, lambda b: (0, 0))
    return pl.pallas_call(
        finish_kernel,
        grid=(rows // size,),
        in_specs=[by_block(inner), by_block(STATE), pl.BlockSpec((heads, size), lambda b: (0, b))]
        + [by_block(inner), whole(state), whole(gain)],
        out_specs=[pl.BlockSpec((size, inner), lambda b: (0, 0))] * 2,
        out_shape=[jax.ShapeDtypeStruct((size, inner), BF)] * 2,
        name="mixer_finish",
    )(y, read, grow, gate, state, gain)


def split_state(packed):
    packed = packed.astype(F32)
    return packed[..., STATE : STATE + 1, :], packed[..., :STATE, :]


def joined(earlier, later):
    return earlier[0] * later[0], earlier[1] * later[0] + later[1]


def packed_state(pair):
    decay = jnp.broadcast_to(pair[0], (RIM, pair[0].shape[1]))
    return jnp.concatenate([pair[1], decay], 0).astype(BF)


def state_before(packed):
    own = split_state(packed)
    other = split_state(swapped(packed))
    late = lax.axis_index("sp_2") == 1
    first = jax.tree.map(lambda a, b: jnp.where(late, a, b), other, own)
    second = jax.tree.map(lambda a, b: jnp.where(late, a, b), own, other)
    running = joined(first, second)
    before = (
        jnp.where(late, other[0], 1.0),
        jnp.where(late, other[1], 0.0),
    )
    for axis in ("sp_1", "sp_0"):
        here = lax.axis_index(axis)
        all_of = sent_to_all(packed_state(running), axis)
        decay, state = split_state(all_of)
        whole = (jnp.ones_like(decay[0]), jnp.zeros_like(state[0]))
        inside = whole
        for k in range(lax.axis_size(axis)):
            whole = joined(whole, (decay[k], state[k]))
            passed = k < here
            inside = jax.tree.map(lambda new, old: jnp.where(passed, new, old), whole, inside)
        before = joined(inside, before)
        running = whole
    return before[1]


def halved_ring(step, top, low):
    result = {}
    for key, value, by in (
        ("bt", top, 1), ("al", low, -1), ("bl", low, 1), ("at", top, -1),
    ):
        result[key] = step(value, by)
    far_top = step(result["bt"], 1)
    far_low = step(result["al"], -1)
    return [
        top, low, result["bt"], result["bl"], result["at"], result["al"], far_top, far_low,
    ]


def rolled(rows, taps):
    count = taps.shape[0]
    result = taps[count - 1 : count] * rows
    for back in range(1, count):
        result = result + taps[count - 1 - back : count - back] * pltpu.roll(rows, back, 0)
    return result


HOPS = (0, -1, 1, 2)


BAND = 512


def go(into, src, dst, sems):
    copy = pltpu.make_async_copy(src, dst, sems.at[len(into)])
    copy.start()
    into.append(copy)


def near_kernel(
    place_ref, p0, l0, p1, l1, p2, l2, halo, res, rim, o0, ob, oa, of, tb, ta, tf,
    total_out,
    x, wo, stream, total, sem_x, sem_o, sem_t,
):
    core = place_ref[2]
    tp_index = place_ref[3]
    rows, width = res.shape
    inner = p0.shape[1]
    half = inner // 2
    near = 3 * inner
    copies_x, copies_o = [], []
    for k, by in enumerate(HOPS):
        at = lax.rem(tp_index + (by + 4), 4)
        columns = pl.ds(k * inner, inner)
        if k < 3:
            top, low = ((p0, l0), (p1, l1), (p2, l2))[k]
            go(copies_x, top, x.at[pl.ds(RIM, rows // 2), columns], sem_x)
            go(copies_x, low, x.at[pl.ds(RIM + rows // 2, rows // 2), columns], sem_x)
        go(copies_x, halo.at[at], x.at[pl.ds(0, RIM), columns], sem_x)
    bands = width // BAND

    def out_weight(n):
        columns = pl.ds(n * BAND, BAND)
        go(copies_o, o0.at[:, columns], wo.at[pl.ds(0, inner), columns], sem_o)
        for side, pieces in ((core, (ob, oa, of)), (1 - core, (tb, ta, tf))):
            first = pl.multiple_of(side * half, half)
            for k, src in enumerate(pieces):
                into = pl.ds((k + 1) * inner + first, half)
                go(copies_o, src.at[:, columns], wo.at[into, columns], sem_o)

    out_weight(0)
    go(copies_x, rim.at[:, pl.ds(rim.shape[1] - width, width)], stream.at[pl.ds(0, RIM)], sem_x)
    go(copies_x, res, stream.at[pl.ds(RIM, rows)], sem_x)
    for n in range(1, bands):
        out_weight(n)
    for copy in copies_x + copies_o:
        copy.wait()

    def store(n):
        columns = pl.ds(n * BAND, BAND)
        return pltpu.make_async_copy(total.at[:, columns], total_out.at[:, columns], sem_t.at[n])

    def band(n, _):
        columns = pl.ds(pl.multiple_of(n * BAND, BAND), BAND)
        total[:, columns] = stream[:, columns].astype(F32) + jnp.dot(
            x[:, :near], wo[:near, columns], preferred_element_type=F32
        )
        total[:RIM, columns] += jnp.dot(
            x[:RIM, near:], wo[near:, columns], preferred_element_type=F32
        )
        store(n).start()
        return 0

    lax.fori_loop(0, bands, band, 0)
    for n in range(bands):
        store(n).wait()


def out_near(place, pieces, halo, residual, rim, out_weights):
    rows, width = residual.shape
    hbm = pl.BlockSpec(memory_space=pl.ANY)
    return pl.pallas_call(
        near_kernel,
        in_specs=[pl.BlockSpec(memory_space=pltpu.SMEM)] + [hbm] * 16,
        out_specs=hbm,
        out_shape=jax.ShapeDtypeStruct((rows + RIM, width), F32),
        scratch_shapes=[
            pltpu.VMEM((rows + RIM, width), BF),
            pltpu.VMEM((width, width), BF),
            pltpu.VMEM((rows + RIM, width), BF),
            pltpu.VMEM((rows + RIM, width), F32),
            pltpu.SemaphoreType.DMA((12,)),
            pltpu.SemaphoreType.DMA((28,)),
            pltpu.SemaphoreType.DMA((4,)),
        ],
        compiler_params=pltpu.CompilerParams(vmem_limit_bytes=60 * 1024 * 1024),
        name="out_near",
    )(place, *pieces, halo, residual, rim, *out_weights)


UNIT = 256


def unit_blocks(units):
    return [(at, min(UNIT, units - at)) for at in range(0, units, UNIT)]


def weight_copies(place_ref, plane, wall, sems, units):
    z_index = place_ref[0]
    y_index = place_ref[1]
    core = place_ref[2]
    every = []
    stretches = ((0, 2 * UNIT), (2 * UNIT, 2 * units), (2 * units, 3 * units))

    def start(stretch):
        lanes = pl.ds(stretches[stretch][0], stretches[stretch][1] - stretches[stretch][0])
        done = len(every)
        for side, sources in ((core, plane[:8]), (1 - core, plane[8:])):
            first_axis = jnp.where(side == 0, y_index, z_index)
            second_axis = jnp.where(side == 0, z_index, y_index)
            for m, by_second in enumerate(HOPS):
                second = lax.rem(second_axis + (by_second + 4), 4)
                for k, by_first in enumerate((0, -1, 1, 2)):
                    first = lax.rem(first_axis + (by_first + 4), 4)
                    chip = jnp.where(side == 0, second * 4 + first, first * 4 + second)
                    src = sources[2 * m + k // 2].at[k % 2, :, :, lanes]
                    go(every, src, wall.at[chip, :, side, :, lanes], sems)
        return every[done:]

    return start


def ffn_blocks(xin, wall, hid, part, tg_ref, tv_ref, arrived, start, stored):
    width = xin.shape[1]
    units = hid.shape[1]
    for j, (at, size) in enumerate(unit_blocks(units)):
        if j < 2:
            for copy in arrived[j]:
                copy.wait()
        if j == 0:
            arrived.append(start(2))
        weight = wall[..., 2 * at : 2 * (at + size)].reshape(width, 2 * size)
        rows = jnp.dot(xin[...], weight, preferred_element_type=F32).astype(BF).astype(F32)
        taps = jnp.concatenate([tg_ref[:, at : at + size], tv_ref[:, at : at + size]], 1)
        rows = rolled(rows, taps.astype(F32))
        act = (silu(rows[:, :size]) * rows[:, size:]).astype(BF)
        hid[:, at : at + size] = act[RIM:]
    for copy in arrived[2]:
        copy.wait()
    bands = width // BAND
    chips = wall.shape[0] // bands

    def band(n, _):
        weight = wall[pl.ds(n * chips, chips), :, :, :, 2 * units :].reshape(BAND, units)
        part[:, pl.ds(pl.multiple_of(n * BAND, BAND), BAND)] = lax.dot_general(
            hid[...], weight, (((1,), (1,)), ((), ())), preferred_element_type=F32
        ).astype(BF)
        stored(n)
        return 0

    lax.fori_loop(0, bands, band, 0)


def ffn_kernel(
    place_ref, p3a, p3b, total_in, of, tf,
    w0, w1, w2, w3, w4, w5, w6, w7, s0, s1, s2, s3, s4, s5, s6, s7,
    gain_ref, tg_ref, tv_ref,
    q0, q1, q3, qa, qb, own_ref,
    p3, wo, total, wall, stream, xin, hid, part, sem_x, sem_t, sem_w, sem_q,
):
    core = place_ref[2]
    tp_index = place_ref[3]
    rows, inner = p3.shape
    width = wo.shape[1]
    units = hid.shape[1]
    half = inner // 2
    share = rows // 4
    bands = width // BAND
    copies_x, copies_t = [], []
    go(copies_x, p3a, p3.at[pl.ds(0, rows // 2)], sem_x)
    go(copies_x, p3b, p3.at[pl.ds(rows // 2, rows // 2)], sem_x)
    go(copies_x, of, wo.at[pl.ds(pl.multiple_of(core * half, half), half)], sem_x)
    go(copies_x, tf, wo.at[pl.ds(pl.multiple_of((1 - core) * half, half), half)], sem_x)
    for n in range(bands):
        columns = pl.ds(n * BAND, BAND)
        go(copies_t, total_in.at[:, columns], total.at[:, columns], sem_t)
    for copy in copies_x:
        copy.wait()
    squares = jnp.zeros((rows + RIM, 1), F32)
    for n in range(bands):
        copies_t[n].wait()
        if n == 1:
            plane = (w0, w1, w2, w3, w4, w5, w6, w7, s0, s1, s2, s3, s4, s5, s6, s7)
            start = weight_copies(place_ref, plane, wall, sem_w, units)
            arrived = [start(0)]
        if n == 2:
            arrived.append(start(1))
        columns = slice(n * BAND, (n + 1) * BAND)
        total[RIM:, columns] += jnp.dot(p3[...], wo[:, columns], preferred_element_type=F32)
        kept = total[:, columns].astype(BF)
        stream[:, columns] = kept
        wide = kept.astype(F32)
        squares = squares + jnp.sum(wide * wide, axis=-1, keepdims=True)
    scale = lax.rsqrt(squares / width + epsilon)
    for n in range(bands):
        columns = slice(n * BAND, (n + 1) * BAND)
        xin[:, columns] = (
            stream[:, columns].astype(F32) * scale * gain_ref[:, columns]
        ).astype(BF)
    own_ref[...] = stream[pl.ds(pl.multiple_of(RIM + tp_index * share, 16), share), :]
    shares = []
    for k, dst in ((2, qa), (2, qb), (1, q1), (3, q3), (0, q0)):
        first = lax.rem(tp_index + k, 4) * share
        if dst is qb:
            first = first + share // 2
        shares.append((pl.multiple_of(first, 16), dst))

    def stores(n):
        columns = pl.ds(n * BAND, BAND)
        return [
            pltpu.make_async_copy(
                part.at[pl.ds(first, dst.shape[0]), columns],
                dst.at[:, columns],
                sem_q.at[n * len(shares) + i],
            )
            for i, (first, dst) in enumerate(shares)
        ]

    def stored(n):
        for copy in stores(n):
            copy.start()

    ffn_blocks(xin, wall, hid, part, tg_ref, tv_ref, arrived, start, stored)
    for n in range(bands):
        for copy in stores(n):
            copy.wait()


def ffn(place, pieces, total, far_weights, weights, gain, tg, tv):
    rows, width = total.shape
    rows = rows - RIM
    inner = pieces[0].shape[1]
    units = tg.shape[1]
    share = rows // 4
    hbm = pl.BlockSpec(memory_space=pl.ANY)
    vmem = pl.BlockSpec(memory_space=pltpu.VMEM)
    shape = jax.ShapeDtypeStruct
    return pl.pallas_call(
        ffn_kernel,
        in_specs=[pl.BlockSpec(memory_space=pltpu.SMEM)] + [hbm] * 21 + [vmem] * 3,
        out_specs=[hbm] * 5 + [vmem],
        out_shape=[shape((share, width), BF)] * 3
        + [
            shape((share // 2, width), BF),
            shape((share // 2, width), BF),
            shape((share, width), BF),
        ],
        scratch_shapes=[
            pltpu.VMEM((rows, inner), BF),
            pltpu.VMEM((inner, width), BF),
            pltpu.VMEM((rows + RIM, width), F32),
            pltpu.VMEM((16, 2, 2, width // 64, 3 * units), BF),
            pltpu.VMEM((rows + RIM, width), BF),
            pltpu.VMEM((rows + RIM, width), BF),
            pltpu.VMEM((rows, units), BF),
            pltpu.VMEM((rows, width), BF),
            pltpu.SemaphoreType.DMA((4,)),
            pltpu.SemaphoreType.DMA((4,)),
            pltpu.SemaphoreType.DMA((96,)),
            pltpu.SemaphoreType.DMA((20,)),
        ],
        compiler_params=pltpu.CompilerParams(vmem_limit_bytes=60 * 1024 * 1024),
        name="ffn",
    )(place, *pieces, total, *far_weights, *weights, gain, tg, tv)


def by_units(gate, value):
    return [
        part[:, at : at + size]
        for at, size in unit_blocks(gate.shape[1])
        for part in (gate, value)
    ]


def on_device(
    mixer_value_projection,
    write_vectors_projected,
    read_vectors_projected,
    output_gate_projected,
    step_size_scores,
    position_decay_extra,
    step_size_bias,
    head_decay_logarithm,
    value_filter_taps,
    write_filter_taps,
    read_filter_taps,
    gated_group_norm_gain,
    mixer_output_weight,
    residual,
    feedforward_norm_gain,
    feedforward_gate_weight,
    feedforward_value_weight,
    gate_filter_taps,
    single_value_filter_taps,
    feedforward_down_weight,
):
    row_count, inner = mixer_value_projection.shape
    core = lax.axis_index("sp_2")
    tp_index = lax.axis_index("tp")

    rows = jnp.concatenate(
        by_units(feedforward_gate_weight, feedforward_value_weight)
        + [feedforward_down_weight.T],
        1,
    )
    part = rows.shape[0] // 2
    keep = jnp.where(core == 0, rows[:part], rows[part:])
    got = swapped(jnp.where(core == 0, rows[part:], rows[:part]))
    piece = jnp.concatenate([jnp.where(core == 0, keep, got), jnp.where(core == 0, got, keep)], 0)
    behind, ahead, far = short_ring(lambda a, by: turned(a, 0, by), piece)
    plane = halved_ring(
        lambda a, by: turned(a, 1, by),
        jnp.concatenate([piece, behind], 0),
        jnp.concatenate([ahead, far], 0),
    )
    plane = [a.reshape(-1, 2, part, a.shape[1]) for a in plane]
    weights = [*plane, *named_swaps(plane)]

    own_half = lax.dynamic_slice_in_dim(mixer_output_weight, core * (inner // 2), inner // 2, 0)
    out_ring = short_ring(lambda a, by: shifted(a, "tp", by, True), own_half)
    out_weights = [mixer_output_weight, *out_ring, *named_swaps(out_ring)]

    rim = jnp.concatenate(
        [
            a[row_count - RIM :]
            for a in (
                mixer_value_projection,
                write_vectors_projected,
                read_vectors_projected,
                residual,
            )
        ],
        1,
    )
    rim = shifted(rim, SP, 1)
    scaled, write, read, entering, cum, grow, packed = mixer_local(
        mixer_value_projection,
        write_vectors_projected.T,
        read_vectors_projected.T,
        rim,
        step_size_scores.T,
        position_decay_extra.T,
        step_size_bias[None],
        head_decay_logarithm[None],
        value_filter_taps,
        write_filter_taps,
        read_filter_taps,
    )
    y = mixer_inside(scaled, write, read, entering, cum)
    state = state_before(packed)
    top, low = mixer_finish(
        y, read, grow, output_gate_projected, state, gated_group_norm_gain[None]
    )
    ring = halved_ring(lambda a, by: shifted(a, "tp", by, True), top, low)
    near, far = ring[:6], ring[6:]
    halo = shifted(low[low.shape[0] - RIM :], SP, 1)
    halo = sent_to_all(halo, "tp")
    places = [lax.axis_index("sp_0"), lax.axis_index("sp_1"), core, tp_index]
    place = jnp.stack(places).astype(jnp.int32)
    total = out_near(place, near, halo, residual, rim, out_weights)
    far_weights = (out_weights[3], out_weights[6])
    here, on, back, far_on, far_back, own = ffn(
        place,
        far,
        total,
        far_weights,
        weights,
        feedforward_norm_gain[None],
        gate_filter_taps,
        single_value_filter_taps,
    )
    more_on = shifted(far_on, "tp", 1, True)
    more_back = shifted(far_back, "tp", -1, True)
    half = far_on.shape[0]
    on = (on.astype(F32) + jnp.pad(more_on.astype(F32), ((0, half), (0, 0)))).astype(BF)
    back = (back.astype(F32) + jnp.pad(more_back.astype(F32), ((half, 0), (0, 0)))).astype(BF)
    from_behind = shifted(on, "tp", 1, True)
    from_ahead = shifted(back, "tp", -1, True)
    down = here.astype(F32) + from_behind.astype(F32) + from_ahead.astype(F32)
    return (own.astype(F32) + down).astype(BF)


def solution(mesh):
    torus = Mesh(mesh.devices.reshape(4, 4, 2, mesh.shape["tp"]), ("sp_0", "sp_1", "sp_2", "tp"))
    in_specs = (
        P(SP, "tp"),
        P(SP, "tp"),
        P(SP, "tp"),
        P(SP, "tp"),
        P(SP, "tp"),
        P(SP, "tp"),
        P("tp"),
        P("tp"),
        P(None, "tp"),
        P(None, "tp"),
        P(None, "tp"),
        P("tp"),
        P("tp", None),
        P(SP, None),
        P(),
        P(SP, "tp"),
        P(SP, "tp"),
        P(None, "tp"),
        P(None, "tp"),
        P("tp", SP),
    )
    out_specs = P(SP_TP, None)

    return jax.shard_map(
        on_device, mesh=torus, in_specs=in_specs, out_specs=out_specs, check_vma=False
    )
```

profile of v0, /device:TPU:1, one launch (start us, length us, event | category | flops | bytes accessed | tf_op | source)
XLA Modules:
  0.0 240.9 jit_solution(15659865090344229787)
XLA Ops:
  0.0 2.3 constant_dynamic-slice_fusion
  2.4 2.0 collective-permute-start.9
  7.5 4.5 %collective-permute-start = (bf16[16,2688]{1,0:T(8,128)(2,1)S(1)}, bf16[16,2688]{1,0:T(8,128)(2,1)S(1)}, u32[]{:S(2)}, u32[]{:S(2)}) collective-permute-start(bf16[16,2688]{1,0:T(8,128)(2,1)S(1)} %concatenate.34), channel_id=1, source_target_pairs={{0,4},{4,8},{8,12},{12,16},{16,20},{20,24},{24,28},{28,32},{32,36}... | collective-permute-start | bytes 258056 | tf_op jit(solution)/shard_map/ppermute | solution.py:28
  14.2 7.6 %mixer_local.1 = (bf16[768,512]{1,0:T(8,128)(2,1)}, bf16[768,64]{1,0:T(8,128)(2,1)}, bf16[768,64]{1,0:T(8,128)(2,1)}, f32[384,512]{1,0:T(8,128)}, f32[8,768]{1,0...) custom-call(bf16[768,512]{1,0:T(8,128)(2,1)} %x_ref.1, bf16[64,768]{1,0:T(8,128)(2,1)} %bitcast.95, ...), custom_call_target="tpu_custom_call" | custom-call | tf_op jit(solution)/shard_map/mixer_local/pallas_call | solution.py:188
  23.4 5.0 %mixer_inside.1.y_ref = f32[768,512]{1,0:T(8,128)} custom-call(bf16[768,512]{1,0:T(8,128)(2,1)} %get-tuple-element.20.scaled_ref, bf16[768,64]{1,0:T(8,128)(2,1)} %get-tuple-element.21.write_ref, bf16[768,64]{1,0:T(8,128)(2,1)} %get-tuple-element.22.read_ref, f32[384,512]{1,0:T(8,128)} %get-tuple-element.23.before_ref, f32[8,768]{1,0:T(8,128)} %get-tuple-element.24.cum_ref), custom_call_target="tpu_custom_call" | custom-call | tf_op jit(solution)/shard_map/mixer_inside/pallas_call | solution.py:264
  29.3 4.9 %all-to-all-start = ((bf16[4,80,512]{2,1,0:T(8,128)(2,1)}), bf16[4,80,512]{2,1,0:T(8,128)(2,1)S(1)}, u32[]{:S(2)}, u32[]{:S(2)}) async-start(bf16[4,80,512]{2,1,0:T(8,128)(2,1)} %broadcast_in_dim.52), calls=%async_computation | async-start | bytes 655360 | tf_op jit(solution)/shard_map/all_to_all | solution.py:62
  34.2 6.3 %all-to-all-done = bf16[4,80,512]{2,1,0:T(8,128)(2,1)S(1)} async-done(((bf16[4,80,512]{2,1,0:T(8,128)(2,1)}), bf16[4,80,512]{2,1,0:T(8,128)(2,1)S(1)}, u32[]{:S(2)}, u32[]{:S(2)}) %all-to-all-start) | async-done | bytes 327712 | tf_op jit(solution)/shard_map/all_to_all | solution.py:62
  41.5 6.7 %all-to-all-start.1 = ((bf16[4,80,512]{2,1,0:T(8,128)(2,1)}), bf16[4,80,512]{2,1,0:T(8,128)(2,1)S(1)}, u32[]{:S(2)}, u32[]{:S(2)}) async-start(bf16[4,80,512]{2,1,0:T(8,128)(2,1)} %broadcast_in_dim.54), calls=%async_computation.1 | async-start | bytes 655360 | tf_op jit(solution)/shard_map/all_to_all | solution.py:62
  49.0 1.5 collective-permute-start.16
  51.7 2.5 %all-to-all-done.1 = bf16[4,80,512]{2,1,0:T(8,128)(2,1)S(1)} async-done(((bf16[4,80,512]{2,1,0:T(8,128)(2,1)}), bf16[4,80,512]{2,1,0:T(8,128)(2,1)S(1)}, u32[]{:S(2)}, u32[]{:S(2)}) %all-to-all-start.1) | async-done | bytes 327712 | tf_op jit(solution)/shard_map/all_to_all | solution.py:62
  55.1 3.7 %mixer_finish.1 = (bf16[384,512]{1,0:T(8,128)(2,1)}, bf16[384,512]{1,0:T(8,128)(2,1)}) custom-call(f32[768,512]{1,0:T(8,128)} %mixer_inside.1.y_ref, bf16[768,64]{1,0:T(8,128)(2,1)} %get-tuple-element.22.read_ref, f32[8,768]{1,0:T(8,128)} %get-tuple-element.25.grow_ref, bf16[768,512]{1,0:T(8,128)(2,1)} %gate_ref.1, f32[64,512]{1,0:T(8,128)} %fusion.3.state_ref, ...), custom_call_target="tpu_custom_call" | custom-call | tf_op jit(solution)/shard_map/mixer_finish/pallas_call | solution.py:302
  59.5 6.8 %collective-permute-start.8 = (bf16[16,512]{1,0:T(8,128)(2,1)S(1)}, bf16[16,512]{1,0:T(8,128)(2,1)S(1)}, u32[]{:S(2)}, u32[]{:S(2)}) collective-permute-start(bf16[16,512]{1,0:T(8,128)(2,1)S(1)} %slice.163), channel_id=1, source_target_pairs={{0,4},{4,8},{8,12},{12,16},{16,20},{20,24},{24,28},{28,32},{32,36}... | collective-permute-start | bytes 49160 | tf_op jit(solution)/shard_map/ppermute | solution.py:28
  69.9 2.6 %collective-permute-start.7 = (bf16[384,512]{1,0:T(8,128)(2,1)S(1)}, bf16[384,512]{1,0:T(8,128)(2,1)S(1)}, u32[]{:S(2)}, u32[]{:S(2)}) collective-permute-start(bf16[384,512]{1,0:T(8,128)(2,1)S(1)} %copy-done.15), channel_id=1, source_target_pairs={{0,3},{1,0},{2,1},{3,2},{4,7},{5,4},{6,5},{7,6},{8,11},{9,8},{10,9... | collective-permute-start | bytes 1179656 | tf_op jit(solution)/shard_map/ppermute | solution.py:28
  72.5 16.8 %collective-permute-done.2.p1 = bf16[384,512]{1,0:T(8,128)(2,1)S(1)} collective-permute-done((bf16[384,512]{1,0:T(8,128)(2,1)}, bf16[384,512]{1,0:T(8,128)(2,1)S(1)}, u32[]{:S(2)}, u32[]{:S(2)}) %collective-permute-start.2) | collective-permute-done | bytes 393248 | tf_op jit(solution)/shard_map/ppermute | solution.py:28
  92.7 8.2 %collective-permute-done.18 = bf16[64,4224]{1,0:T(8,128)(2,1)S(1)} collective-permute-done((bf16[64,4224]{1,0:T(8,128)(2,1)}, bf16[64,4224]{1,0:T(8,128)(2,1)S(1)}, u32[]{:S(2)}, u32[]{:S(2)}) %collective-permute-start.18) | collective-permute-done | bytes 540704 | tf_op jit(solution)/shard_map/ppermute | solution.py:43
  101.1 3.4 %collective-permute-done.3.p3a = bf16[384,512]{1,0:T(8,128)(2,1)S(1)} collective-permute-done((bf16[384,512]{1,0:T(8,128)(2,1)S(1)}, bf16[384,512]{1,0:T(8,128)(2,1)S(1)}, u32[]{:S(2)}, u32[]{:S(2)}) %collective-permute-start.3) | collective-permute-done | bytes 393248 | tf_op jit(solution)/shard_map/ppermute | solution.py:28
  104.4 2.7 %collective-permute-start.22 = (bf16[128,4224]{1,0:T(8,128)(2,1)S(1)}, bf16[128,4224]{1,0:T(8,128)(2,1)}, u32[]{:S(2)}, u32[]{:S(2)}) collective-permute-start(bf16[128,4224]{1,0:T(8,128)(2,1)S(1)} %constant_dynamic-update-slice_fusion.12), channel_id=1, source_target_pairs={{0,96},{4,28},{8,104},{12,4},{16,112},{20,12},{24,120},{28,20},{32... | collective-permute-start | bytes 3244040 | tf_op jit(solution)/shard_map/ppermute | solution.py:43
  107.1 3.7 %collective-permute-done.5.p3b = bf16[384,512]{1,0:T(8,128)(2,1)S(1)} collective-permute-done((bf16[384,512]{1,0:T(8,128)(2,1)S(1)}, bf16[384,512]{1,0:T(8,128)(2,1)S(1)}, u32[]{:S(2)}, u32[]{:S(2)}) %collective-permute-start.5) | collective-permute-done | bytes 393248 | tf_op jit(solution)/shard_map/ppermute | solution.py:28
  110.9 1.7 collective-permute-start.12
  112.7 22.4 %collective-permute-done.11.of = bf16[256,2048]{1,0:T(8,128)(2,1)S(1)} collective-permute-done((bf16[256,2048]{1,0:T(8,128)(2,1)S(1)}, bf16[256,2048]{1,0:T(8,128)(2,1)S(1)}, u32[]{:S(2)}, u32[]{:S(2)}) %collective-permute-start.11) | collective-permute-done | bytes 1048608 | tf_op jit(solution)/shard_map/ppermute | solution.py:28
  135.1 2.5 %collective-permute-start.26 = (bf16[2,2,32,4224]{3,2,1,0:T(8,128)(2,1)S(1)}, bf16[2,2,32,4224]{3,2,1,0:T(8,128)(2,1)S(1)}, u32[]{:S(2)}, u32[]{:S(2)}) collective-permute-start(bf16[2,2,32,4224]{3,2,1,0:T(8,128)(2,1)S(1)} %bitcast.91), channel_id=1, source_target_pairs={{0,4},{4,0},{1,5},{5,1},{2,6},{6,2},{3,7},{7,3},{8,12},{12,8},{9,1... | collective-permute-start | bytes 3244040 | tf_op jit(solution)/shard_map/ppermute | solution.py:32
  139.7 2.5 %collective-permute-start.24 = (bf16[128,4224]{1,0:T(8,128)(2,1)}, bf16[128,4224]{1,0:T(8,128)(2,1)}, u32[]{:S(2)}, u32[]{:S(2)}) collective-permute-start(bf16[128,4224]{1,0:T(8,128)(2,1)} %collective-permute-done.22), channel_id=1, source_target_pairs={{0,96},{4,28},{8,104},{12,4},{16,112},{20,12},{24,120},{28,20},{32... | collective-permute-start | bytes 3244040 | tf_op jit(solution)/shard_map/ppermute | solution.py:43
  142.7 10.5 %collective-permute-done.23 = bf16[128,4224]{1,0:T(8,128)(2,1)} collective-permute-done((bf16[128,4224]{1,0:T(8,128)(2,1)S(1)}, bf16[128,4224]{1,0:T(8,128)(2,1)}, u32[]{:S(2)}, u32[]{:S(2)}) %collective-permute-start.23) | collective-permute-done | bytes 1081376 | tf_op jit(solution)/shard_map/ppermute | solution.py:43
  156.4 3.3 %all-to-all-start.2 = ((bf16[4,16,512]{2,1,0:T(8,128)(2,1)}), bf16[4,16,512]{2,1,0:T(8,128)(2,1)S(1)}, u32[]{:S(2)}, u32[]{:S(2)}) async-start(bf16[4,16,512]{2,1,0:T(8,128)(2,1)} %broadcast_in_dim.58), calls=%async_computation.2 | async-start | bytes 131072 | tf_op jit(solution)/shard_map/all_to_all | solution.py:62
  160.3 3.8 %all-to-all-done.2.halo = bf16[4,16,512]{2,1,0:T(8,128)(2,1)S(1)} async-done(((bf16[4,16,512]{2,1,0:T(8,128)(2,1)}), bf16[4,16,512]{2,1,0:T(8,128)(2,1)S(1)}, u32[]{:S(2)}, u32[]{:S(2)}) %all-to-all-start.2) | async-done | bytes 65568 | tf_op jit(solution)/shard_map/all_to_all | solution.py:62
  164.7 13.3 %out_near.1.total_in = f32[784,2048]{1,0:T(8,128)} custom-call(s32[4]{0:T(128)} %pad_add_fusion.place_ref, bf16[384,512]{1,0:T(8,128)(2,1)} %get-tuple-element.27.p0, bf16[384,512]{1,0:T(8,128)(2,1)} %get-tuple-element.28.l0, bf16[384,512]{1,0:T(8,128)(2,1)} %copy-done.18, bf16[384,512]{1,0:T(8,128)(2,1)} %copy-done.17, bf16[384,512]{1,0:T(8,128)(2,1)} %copy-done.19, ...), custom_call_target="tpu_custom_call" | custom-call | tf_op jit(solution)/shard_map/out_near/pallas_call | solution.py:448
  178.1 30.9 %ffn.1 = (bf16[192,2048]{1,0:T(8,128)(2,1)}, bf16[192,2048]{1,0:T(8,128)(2,1)}, bf16[192,2048]{1,0:T(8,128)(2,1)}, bf16[96,2048]{1,0:T(8,128)(2,1)}, bf16[96,204...) custom-call(s32[4]{0:T(128)} %pad_add_fusion.place_ref, bf16[384,512]{1,0:T(8,128)(2,1)} %copy-done.20, ...), custom_call_target="tpu_custom_call" | custom-call | tf_op jit(solution)/shard_map/ffn/pallas_call | solution.py:614
  209.3 2.4 collective-permute-start.35
  211.7 8.2 %collective-permute-done.33 = bf16[96,2048]{1,0:T(8,128)(2,1)S(1)} collective-permute-done((bf16[96,2048]{1,0:T(8,128)(2,1)}, bf16[96,2048]{1,0:T(8,128)(2,1)S(1)}, u32[]{:S(2)}, u32[]{:S(2)}) %collective-permute-start.33) | collective-permute-done | bytes 393248 | tf_op jit(solution)/shard_map/ppermute | solution.py:28
  221.5 2.7 %collective-permute-start.36 = (bf16[192,2048]{1,0:T(8,128)(2,1)S(1)}, bf16[192,2048]{1,0:T(8,128)(2,1)S(1)}, u32[]{:S(2)}, u32[]{:S(2)}) collective-permute-start(bf16[192,2048]{1,0:T(8,128)(2,1)S(1)} %add_convert_fusion.1), channel_id=1, source_target_pairs={{0,3},{1,0},{2,1},{3,2},{4,7},{5,4},{6,5},{7,6},{8,11},{9,8},{10,9... | collective-permute-start | bytes 2359304 | tf_op jit(solution)/shard_map/ppermute | solution.py:28
  224.2 15.4 %collective-permute-done.34 = bf16[192,2048]{1,0:T(8,128)(2,1)S(1)} collective-permute-done((bf16[192,2048]{1,0:T(8,128)(2,1)S(1)}, bf16[192,2048]{1,0:T(8,128)(2,1)S(1)}, u32[]{:S(2)}, u32[]{:S(2)}) %collective-permute-start.34) | collective-permute-done | bytes 786464 | tf_op jit(solution)/shard_map/ppermute | solution.py:28
  239.5 1.4 add_convert_fusion
  (161 shorter events, 28.0 us)
Async XLA Ops:
  2.4 67.5 %collective-permute-start.9 = (bf16[256,2048]{1,0:T(8,128)(2,1)}, bf16[256,2048]{1,0:T(8,128)(2,1)S(1)}, u32[]{:S(2)}, u32[]{:S(2)}) collective-permute-start(bf16[256,2048]{1,0:T(8,128)(2,1)} %constant_dynamic-slice_fusion), channel_id=1, source_target_pairs={{0,1},{1,2},{2,3},{3,0},{4,5},{5,6},{6,7},{7,4},{8,9},{9,10},{10,1... | collective-permute-start | bytes 3145736 | tf_op jit(solution)/shard_map/ppermute | solution.py:28
  4.4 68.1 %collective-permute-start.10 = (bf16[256,2048]{1,0:T(8,128)(2,1)}, bf16[256,2048]{1,0:T(8,128)(2,1)}, u32[]{:S(2)}, u32[]{:S(2)}) collective-permute-start(bf16[256,2048]{1,0:T(8,128)(2,1)} %constant_dynamic-slice_fusion), channel_id=1, source_target_pairs={{0,3},{1,0},{2,1},{3,2},{4,7},{5,4},{6,5},{7,6},{8,11},{9,8},{10,9... | collective-permute-start | bytes 3145736 | tf_op jit(solution)/shard_map/ppermute | solution.py:28
  22.0 12.2 %collective-permute-start.15 = (bf16[32,4224]{1,0:T(8,128)(2,1)S(1)}, bf16[32,4224]{1,0:T(8,128)(2,1)S(1)}, u32[]{:S(2)}, u32[]{:S(2)}) collective-permute-start(bf16[32,4224]{1,0:T(8,128)(2,1)S(1)} %broadcast_select_fusion.2), channel_id=1, source_target_pairs={{0,4},{4,0},{1,5},{5,1},{2,6},{6,2},{3,7},{7,3},{8,12},{12,8},{9,1... | collective-permute-start | bytes 811016 | tf_op jit(solution)/shard_map/ppermute | solution.py:32
  29.3 11.3 %all-to-all-start = ((bf16[4,80,512]{2,1,0:T(8,128)(2,1)}), bf16[4,80,512]{2,1,0:T(8,128)(2,1)S(1)}, u32[]{:S(2)}, u32[]{:S(2)}) async-start(bf16[4,80,512]{2,1,0:T(8,128)(2,1)} %broadcast_in_dim.52), calls=%async_computation | async-start | bytes 655360 | tf_op jit(solution)/shard_map/all_to_all | solution.py:62
  41.5 12.6 %all-to-all-start.1 = ((bf16[4,80,512]{2,1,0:T(8,128)(2,1)}), bf16[4,80,512]{2,1,0:T(8,128)(2,1)S(1)}, u32[]{:S(2)}, u32[]{:S(2)}) async-start(bf16[4,80,512]{2,1,0:T(8,128)(2,1)} %broadcast_in_dim.54), calls=%async_computation.1 | async-start | bytes 655360 | tf_op jit(solution)/shard_map/all_to_all | solution.py:62
  49.0 19.4 %collective-permute-start.16 = (bf16[64,4224]{1,0:T(8,128)(2,1)}, bf16[64,4224]{1,0:T(8,128)(2,1)}, u32[]{:S(2)}, u32[]{:S(2)}) collective-permute-start(bf16[64,4224]{1,0:T(8,128)(2,1)} %pad_maximum_fusion.1), channel_id=1, source_target_pairs={{0,8},{4,36},{8,16},{12,44},{16,24},{20,52},{24,0},{28,60},{32,40}... | collective-permute-start | bytes 1622024 | tf_op jit(solution)/shard_map/ppermute | solution.py:43
  50.5 18.1 %collective-permute-start.17 = (bf16[64,4224]{1,0:T(8,128)(2,1)}, bf16[64,4224]{1,0:T(8,128)(2,1)}, u32[]{:S(2)}, u32[]{:S(2)}) collective-permute-start(bf16[64,4224]{1,0:T(8,128)(2,1)} %pad_maximum_fusion.1), channel_id=1, source_target_pairs={{0,24},{4,100},{8,0},{12,108},{16,8},{20,116},{24,16},{28,124},{32... | collective-permute-start | bytes 1622024 | tf_op jit(solution)/shard_map/ppermute | solution.py:43
  67.1 23.3 %collective-permute-start.4 = (bf16[384,512]{1,0:T(8,128)(2,1)}, bf16[384,512]{1,0:T(8,128)(2,1)S(1)}, u32[]{:S(2)}, u32[]{:S(2)}) collective-permute-start(bf16[384,512]{1,0:T(8,128)(2,1)} %get-tuple-element.28.l0), channel_id=1, source_target_pairs={{0,3},{1,0},{2,1},{3,2},{4,7},{5,4},{6,5},{7,6},{8,11},{9,8},{10,9... | collective-permute-start | bytes 1179656 | tf_op jit(solution)/shard_map/ppermute | solution.py:28
  68.4 22.6 %collective-permute-start.6 = (bf16[384,512]{1,0:T(8,128)(2,1)}, bf16[384,512]{1,0:T(8,128)(2,1)S(1)}, u32[]{:S(2)}, u32[]{:S(2)}) collective-permute-start(bf16[384,512]{1,0:T(8,128)(2,1)} %get-tuple-element.28.l0), channel_id=1, source_target_pairs={{0,1},{1,2},{2,3},{3,0},{4,5},{5,6},{6,7},{7,4},{8,9},{9,10},{10,1... | collective-permute-start | bytes 1179656 | tf_op jit(solution)/shard_map/ppermute | solution.py:28
  68.6 20.7 %collective-permute-start.2 = (bf16[384,512]{1,0:T(8,128)(2,1)}, bf16[384,512]{1,0:T(8,128)(2,1)S(1)}, u32[]{:S(2)}, u32[]{:S(2)}) collective-permute-start(bf16[384,512]{1,0:T(8,128)(2,1)} %get-tuple-element.27.p0), channel_id=1, source_target_pairs={{0,1},{1,2},{2,3},{3,0},{4,5},{5,6},{6,7},{7,4},{8,9},{9,10},{10,1... | collective-permute-start | bytes 1179656 | tf_op jit(solution)/shard_map/ppermute | solution.py:28
  69.9 22.7 %collective-permute-start.7 = (bf16[384,512]{1,0:T(8,128)(2,1)S(1)}, bf16[384,512]{1,0:T(8,128)(2,1)S(1)}, u32[]{:S(2)}, u32[]{:S(2)}) collective-permute-start(bf16[384,512]{1,0:T(8,128)(2,1)S(1)} %copy-done.15), channel_id=1, source_target_pairs={{0,3},{1,0},{2,1},{3,2},{4,7},{5,4},{6,5},{7,6},{8,11},{9,8},{10,9... | collective-permute-start | bytes 1179656 | tf_op jit(solution)/shard_map/ppermute | solution.py:28
  72.5 38.3 %collective-permute-start.19 = (bf16[128,4224]{1,0:T(8,128)(2,1)S(1)}, bf16[128,4224]{1,0:T(8,128)(2,1)S(1)}, u32[]{:S(2)}, u32[]{:S(2)}) collective-permute-start(bf16[128,4224]{1,0:T(8,128)(2,1)S(1)} %pad_maximum_fusion), channel_id=1, source_target_pairs={{0,32},{4,12},{8,40},{12,20},{16,48},{20,28},{24,56},{28,4},{32,64... | collective-permute-start | bytes 3244040 | tf_op jit(solution)/shard_map/ppermute | solution.py:43
  89.3 23.3 %collective-permute-start.21 = (bf16[128,4224]{1,0:T(8,128)(2,1)S(1)}, bf16[128,4224]{1,0:T(8,128)(2,1)}, u32[]{:S(2)}, u32[]{:S(2)}) collective-permute-start(bf16[128,4224]{1,0:T(8,128)(2,1)S(1)} %pad_maximum_fusion), channel_id=1, source_target_pairs={{0,96},{4,28},{8,104},{12,4},{16,112},{20,12},{24,120},{28,20},{32... | collective-permute-start | bytes 3244040 | tf_op jit(solution)/shard_map/ppermute | solution.py:43
  90.4 22.3 %collective-permute-start.25 = (bf16[2,2,32,4224]{3,2,1,0:T(8,128)(2,1)S(1)}, bf16[2,2,32,4224]{3,2,1,0:T(8,128)(2,1)S(1)}, u32[]{:S(2)}, u32[]{:S(2)}) collective-permute-start(bf16[2,2,32,4224]{3,2,1,0:T(8,128)(2,1)S(1)} %bitcast.89), channel_id=1, source_target_pairs={{0,4},{4,0},{1,5},{5,1},{2,6},{6,2},{3,7},{7,3},{8,12},{12,8},{9,1... | collective-permute-start | bytes 3244040 | tf_op jit(solution)/shard_map/ppermute | solution.py:32
  92.6 11.8 %collective-permute-start.3 = (bf16[384,512]{1,0:T(8,128)(2,1)S(1)}, bf16[384,512]{1,0:T(8,128)(2,1)S(1)}, u32[]{:S(2)}, u32[]{:S(2)}) collective-permute-start(bf16[384,512]{1,0:T(8,128)(2,1)S(1)} %collective-permute-done.2.p1), channel_id=1, source_target_pairs={{0,1},{1,2},{2,3},{3,0},{4,5},{5,6},{6,7},{7,4},{8,9},{9,10},{10,1... | collective-permute-start | bytes 1179656 | tf_op jit(solution)/shard_map/ppermute | solution.py:28
  104.4 35.3 %collective-permute-start.22 = (bf16[128,4224]{1,0:T(8,128)(2,1)S(1)}, bf16[128,4224]{1,0:T(8,128)(2,1)}, u32[]{:S(2)}, u32[]{:S(2)}) collective-permute-start(bf16[128,4224]{1,0:T(8,128)(2,1)S(1)} %constant_dynamic-update-slice_fusion.12), channel_id=1, source_target_pairs={{0,96},{4,28},{8,104},{12,4},{16,112},{20,12},{24,120},{28,20},{32... | collective-permute-start | bytes 3244040 | tf_op jit(solution)/shard_map/ppermute | solution.py:43
  110.9 24.3 %collective-permute-start.11 = (bf16[256,2048]{1,0:T(8,128)(2,1)S(1)}, bf16[256,2048]{1,0:T(8,128)(2,1)S(1)}, u32[]{:S(2)}, u32[]{:S(2)}) collective-permute-start(bf16[256,2048]{1,0:T(8,128)(2,1)S(1)} %copy-done.9), channel_id=1, source_target_pairs={{0,1},{1,2},{2,3},{3,0},{4,5},{5,6},{6,7},{7,4},{8,9},{9,10},{10,1... | collective-permute-start | bytes 3145736 | tf_op jit(solution)/shard_map/ppermute | solution.py:28
  110.9 26.8 %collective-permute-start.12 = (bf16[256,2048]{1,0:T(8,128)(2,1)S(1)}, bf16[256,2048]{1,0:T(8,128)(2,1)S(1)}, u32[]{:S(2)}, u32[]{:S(2)}) collective-permute-start(bf16[256,2048]{1,0:T(8,128)(2,1)S(1)} %copy-done.9), channel_id=1, source_target_pairs={{0,4},{4,0},{1,5},{5,1},{2,6},{6,2},{3,7},{7,3},{8,12},{12,8},{9,1... | collective-permute-start | bytes 3145736 | tf_op jit(solution)/shard_map/ppermute | solution.py:32
  112.6 25.8 %collective-permute-start.13 = (bf16[256,2048]{1,0:T(8,128)(2,1)}, bf16[256,2048]{1,0:T(8,128)(2,1)S(1)}, u32[]{:S(2)}, u32[]{:S(2)}) collective-permute-start(bf16[256,2048]{1,0:T(8,128)(2,1)} %collective-permute-done.10.oa), channel_id=1, source_target_pairs={{0,4},{4,0},{1,5},{5,1},{2,6},{6,2},{3,7},{7,3},{8,12},{12,8},{9,1... | collective-permute-start | bytes 3145736 | tf_op jit(solution)/shard_map/ppermute | solution.py:32
  112.7 29.5 %collective-permute-start.20 = (bf16[128,4224]{1,0:T(8,128)(2,1)S(1)}, bf16[128,4224]{1,0:T(8,128)(2,1)}, u32[]{:S(2)}, u32[]{:S(2)}) collective-permute-start(bf16[128,4224]{1,0:T(8,128)(2,1)S(1)} %constant_dynamic-update-slice_fusion.12), channel_id=1, source_target_pairs={{0,32},{4,12},{8,40},{12,20},{16,48},{20,28},{24,56},{28,4},{32,64... | collective-permute-start | bytes 3244040 | tf_op jit(solution)/shard_map/ppermute | solution.py:43
  137.6 15.6 %collective-permute-start.23 = (bf16[128,4224]{1,0:T(8,128)(2,1)S(1)}, bf16[128,4224]{1,0:T(8,128)(2,1)}, u32[]{:S(2)}, u32[]{:S(2)}) collective-permute-start(bf16[128,4224]{1,0:T(8,128)(2,1)S(1)} %collective-permute-done.19), channel_id=1, source_target_pairs={{0,32},{4,12},{8,40},{12,20},{16,48},{20,28},{24,56},{28,4},{32,64... | collective-permute-start | bytes 3244040 | tf_op jit(solution)/shard_map/ppermute | solution.py:43
  139.7 14.5 %collective-permute-start.27 = (bf16[2,2,32,4224]{3,2,1,0:T(8,128)(2,1)S(1)}, bf16[2,2,32,4224]{3,2,1,0:T(8,128)(2,1)S(1)}, u32[]{:S(2)}, u32[]{:S(2)}) collective-permute-start(bf16[2,2,32,4224]{3,2,1,0:T(8,128)(2,1)S(1)} %bitcast.93), channel_id=1, source_target_pairs={{0,4},{4,0},{1,5},{5,1},{2,6},{6,2},{3,7},{7,3},{8,12},{12,8},{9,1... | collective-permute-start | bytes 3244040 | tf_op jit(solution)/shard_map/ppermute | solution.py:32
  139.7 15.1 %collective-permute-start.24 = (bf16[128,4224]{1,0:T(8,128)(2,1)}, bf16[128,4224]{1,0:T(8,128)(2,1)}, u32[]{:S(2)}, u32[]{:S(2)}) collective-permute-start(bf16[128,4224]{1,0:T(8,128)(2,1)} %collective-permute-done.22), channel_id=1, source_target_pairs={{0,96},{4,28},{8,104},{12,4},{16,112},{20,12},{24,120},{28,20},{32... | collective-permute-start | bytes 3244040 | tf_op jit(solution)/shard_map/ppermute | solution.py:43
  142.2 12.1 %collective-permute-start.14 = (bf16[256,2048]{1,0:T(8,128)(2,1)S(1)}, bf16[256,2048]{1,0:T(8,128)(2,1)S(1)}, u32[]{:S(2)}, u32[]{:S(2)}) collective-permute-start(bf16[256,2048]{1,0:T(8,128)(2,1)S(1)} %collective-permute-done.11.of), channel_id=1, source_target_pairs={{0,4},{4,0},{1,5},{5,1},{2,6},{6,2},{3,7},{7,3},{8,12},{12,8},{9,1... | collective-permute-start | bytes 3145736 | tf_op jit(solution)/shard_map/ppermute | solution.py:32
  142.2 35.8 %collective-permute-start.29 = (bf16[2,2,32,4224]{3,2,1,0:T(8,128)(2,1)}, bf16[2,2,32,4224]{3,2,1,0:T(8,128)(2,1)}, u32[]{:S(2)}, u32[]{:S(2)}) collective-permute-start(bf16[2,2,32,4224]{3,2,1,0:T(8,128)(2,1)} %bitcast.37.w4), channel_id=1, source_target_pairs={{0,4},{4,0},{1,5},{5,1},{2,6},{6,2},{3,7},{7,3},{8,12},{12,8},{9,1... | collective-permute-start | bytes 3244040 | tf_op jit(solution)/shard_map/ppermute | solution.py:32
  153.3 24.8 %collective-permute-start.30 = (bf16[2,2,32,4224]{3,2,1,0:T(8,128)(2,1)}, bf16[2,2,32,4224]{3,2,1,0:T(8,128)(2,1)}, u32[]{:S(2)}, u32[]{:S(2)}) collective-permute-start(bf16[2,2,32,4224]{3,2,1,0:T(8,128)(2,1)} %bitcast.38.w5), channel_id=1, source_target_pairs={{0,4},{4,0},{1,5},{5,1},{2,6},{6,2},{3,7},{7,3},{8,12},{12,8},{9,1... | collective-permute-start | bytes 3244040 | tf_op jit(solution)/shard_map/ppermute | solution.py:32
  154.2 23.8 %collective-permute-start.28 = (bf16[2,2,32,4224]{3,2,1,0:T(8,128)(2,1)}, bf16[2,2,32,4224]{3,2,1,0:T(8,128)(2,1)}, u32[]{:S(2)}, u32[]{:S(2)}) collective-permute-start(bf16[2,2,32,4224]{3,2,1,0:T(8,128)(2,1)} %bitcast.36.w3), channel_id=1, source_target_pairs={{0,4},{4,0},{1,5},{5,1},{2,6},{6,2},{3,7},{7,3},{8,12},{12,8},{9,1... | collective-permute-start | bytes 3244040 | tf_op jit(solution)/shard_map/ppermute | solution.py:32
  154.3 23.8 %collective-permute-start.31 = (bf16[2,2,32,4224]{3,2,1,0:T(8,128)(2,1)}, bf16[2,2,32,4224]{3,2,1,0:T(8,128)(2,1)}, u32[]{:S(2)}, u32[]{:S(2)}) collective-permute-start(bf16[2,2,32,4224]{3,2,1,0:T(8,128)(2,1)} %bitcast.39.w6), channel_id=1, source_target_pairs={{0,4},{4,0},{1,5},{5,1},{2,6},{6,2},{3,7},{7,3},{8,12},{12,8},{9,1... | collective-permute-start | bytes 3244040 | tf_op jit(solution)/shard_map/ppermute | solution.py:32
  155.2 22.9 %collective-permute-start.32 = (bf16[2,2,32,4224]{3,2,1,0:T(8,128)(2,1)}, bf16[2,2,32,4224]{3,2,1,0:T(8,128)(2,1)}, u32[]{:S(2)}, u32[]{:S(2)}) collective-permute-start(bf16[2,2,32,4224]{3,2,1,0:T(8,128)(2,1)} %bitcast.40.w7), channel_id=1, source_target_pairs={{0,4},{4,0},{1,5},{5,1},{2,6},{6,2},{3,7},{7,3},{8,12},{12,8},{9,1... | collective-permute-start | bytes 3244040 | tf_op jit(solution)/shard_map/ppermute | solution.py:32
  209.3 12.0 %collective-permute-start.35 = (bf16[96,2048]{1,0:T(8,128)(2,1)}, bf16[96,2048]{1,0:T(8,128)(2,1)S(1)}, u32[]{:S(2)}, u32[]{:S(2)}) collective-permute-start(bf16[96,2048]{1,0:T(8,128)(2,1)} %get-tuple-element.34), channel_id=1, source_target_pairs={{0,3},{1,0},{2,1},{3,2},{4,7},{5,4},{6,5},{7,6},{8,11},{9,8},{10,9... | collective-permute-start | bytes 1179656 | tf_op jit(solution)/shard_map/ppermute | solution.py:28
  221.2 18.3 %collective-permute-start.34 = (bf16[192,2048]{1,0:T(8,128)(2,1)S(1)}, bf16[192,2048]{1,0:T(8,128)(2,1)S(1)}, u32[]{:S(2)}, u32[]{:S(2)}) collective-permute-start(bf16[192,2048]{1,0:T(8,128)(2,1)S(1)} %add_convert_fusion.2), channel_id=1, source_target_pairs={{0,1},{1,2},{2,3},{3,0},{4,5},{5,6},{6,7},{7,4},{8,9},{9,10},{10,1... | collective-permute-start | bytes 2359304 | tf_op jit(solution)/shard_map/ppermute | solution.py:28
  221.5 18.1 %collective-permute-start.36 = (bf16[192,2048]{1,0:T(8,128)(2,1)S(1)}, bf16[192,2048]{1,0:T(8,128)(2,1)S(1)}, u32[]{:S(2)}, u32[]{:S(2)}) collective-permute-start(bf16[192,2048]{1,0:T(8,128)(2,1)S(1)} %add_convert_fusion.1), channel_id=1, source_target_pairs={{0,3},{1,0},{2,1},{3,2},{4,7},{5,4},{6,5},{7,6},{8,11},{9,8},{10,9... | collective-permute-start | bytes 2359304 | tf_op jit(solution)/shard_map/ppermute | solution.py:28
  (37 other events, 650.4 us)
where the time goes:
time: 244 us; the launch traced here: 241 us
  waiting for transfers between devices  103 us (42%)
  Pallas kernels  60.5 us (25%)
  starting transfers between devices  57.6 us (24%)
  local copies, waits for them, and re-layouts  11.3 us (5%)
  other arithmetic  7.47 us (3%)
    ppermute x15, waiting for transfers between devices, shifted(): return lax.ppermute(value, axis, pairs)  72 us
    pallas_call x1, Pallas kernels, ffn(): pl.pallas_call(ffn_kernel, in_specs=[pl.BlockSpec(memory_space=pltpu.SMEM...  30.9 us
    ppermute x15, starting transfers between devices, shifted(): return lax.ppermute(value, axis, pairs)  24.4 us
    ppermute x9, waiting for transfers between devices, turned(): return lax.ppermute(value, SP, pairs)  18.8 us
    all_to_all x3, starting transfers between devices, sent_to_all(): lax.all_to_all(jnp.broadcast_to(value[None], (length, *value.shape)), axi...  14.8 us
    pallas_call x1, Pallas kernels, out_near(): pl.pallas_call(near_kernel, in_specs=[pl.BlockSpec(memory_space=pltpu.SME...  13.3 us
    all_to_all x3, waiting for transfers between devices, sent_to_all(): lax.all_to_all(jnp.broadcast_to(value[None], (length, *value.shape)), axi...  12.6 us
    ppermute x9, starting transfers between devices, turned(): return lax.ppermute(value, SP, pairs)  10.3 us
  transfers between devices with their start and end apart: 40, of which 13 were waited for; matrix products, arithmetic and copies ran while one was open for 5% of the time, Pallas kernels for 12%

commit v1 on v0

--- a/solution.py
+++ b/solution.py
@@ -419,7 +419,7 @@
     go(copies_x, res, stream.at[pl.ds(RIM, rows)], sem_x)
     for n in range(1, bands):
         out_weight(n)
-    for copy in copies_x + copies_o:
+    for copy in copies_x + copies_o[:7]:
         copy.wait()
 
     def store(n):
@@ -427,7 +427,7 @@
         return pltpu.make_async_copy(total.at[:, columns], total_out.at[:, columns], sem_t.at[n])
 
     def band(n, _):
-        columns = pl.ds(pl.multiple_of(n * BAND, BAND), BAND)
+        columns = pl.ds(n * BAND if isinstance(n, int) else pl.multiple_of(n * BAND, BAND), BAND)
         total[:, columns] = stream[:, columns].astype(F32) + jnp.dot(
             x[:, :near], wo[:near, columns], preferred_element_type=F32
         )
@@ -437,7 +437,10 @@
         store(n).start()
         return 0
 
-    lax.fori_loop(0, bands, band, 0)
+    band(0, 0)
+    for copy in copies_o[7:]:
+        copy.wait()
+    lax.fori_loop(1, bands, band, 0)
     for n in range(bands):
         store(n).wait()
 

time: 244 us -> 244 us (level)
  no operation moved by 1% of the time
where the time goes in v1:
time: 244 us; the launch traced here: 241 us
  waiting for transfers between devices  103 us (42%)
  Pallas kernels  60.5 us (25%)
  starting transfers between devices  57.6 us (24%)
  local copies, waits for them, and re-layouts  11.3 us (5%)
  other arithmetic  7.47 us (3%)
    ppermute x15, waiting for transfers between devices, shifted(): return lax.ppermute(value, axis, pairs)  72 us
    pallas_call x1, Pallas kernels, ffn(): pl.pallas_call(ffn_kernel, in_specs=[pl.BlockSpec(memory_space=pltpu.SMEM...  30.9 us
    ppermute x15, starting transfers between devices, shifted(): return lax.ppermute(value, axis, pairs)  24.4 us
    ppermute x9, waiting for transfers between devices, turned(): return lax.ppermute(value, SP, pairs)  18.8 us
    all_to_all x3, starting transfers between devices, sent_to_all(): lax.all_to_all(jnp.broadcast_to(value[None], (length, *value.shape)), axi...  14.8 us
    pallas_call x1, Pallas kernels, out_near(): pl.pallas_call(near_kernel, in_specs=[pl.BlockSpec(memory_space=pltpu.SME...  13.3 us
    all_to_all x3, waiting for transfers between devices, sent_to_all(): lax.all_to_all(jnp.broadcast_to(value[None], (length, *value.shape)), axi...  12.6 us
    ppermute x9, starting transfers between devices, turned(): return lax.ppermute(value, SP, pairs)  10.3 us
  transfers between devices with their start and end apart: 40, of which 13 were waited for; matrix products, arithmetic and copies ran while one was open for 5% of the time, Pallas kernels for 12%

profile of v1, /device:TPU:1, one launch (start us, length us, event | category | flops | bytes accessed | tf_op | source)
XLA Modules:
  0.0 240.9 jit_solution(11547321493326790638)
XLA Ops:
  0.0 2.3 constant_dynamic-slice_fusion
  2.4 2.0 collective-permute-start.9
  7.5 4.5 %collective-permute-start = (bf16[16,2688]{1,0:T(8,128)(2,1)S(1)}, bf16[16,2688]{1,0:T(8,128)(2,1)S(1)}, u32[]{:S(2)}, u32[]{:S(2)}) collective-permute-start(bf16[16,2688]{1,0:T(8,128)(2,1)S(1)} %concatenate.34), channel_id=1, source_target_pairs={{0,4},{4,8},{8,12},{12,16},{16,20},{20,24},{24,28},{28,32},{32,36}... | collective-permute-start | bytes 258056 | tf_op jit(solution)/shard_map/ppermute | solution.py:28
  14.2 7.6 %mixer_local.1 = (bf16[768,512]{1,0:T(8,128)(2,1)}, bf16[768,64]{1,0:T(8,128)(2,1)}, bf16[768,64]{1,0:T(8,128)(2,1)}, f32[384,512]{1,0:T(8,128)}, f32[8,768]{1,0...) custom-call(bf16[768,512]{1,0:T(8,128)(2,1)} %x_ref.1, bf16[64,768]{1,0:T(8,128)(2,1)} %bitcast.95, ...), custom_call_target="tpu_custom_call" | custom-call | tf_op jit(solution)/shard_map/mixer_local/pallas_call | solution.py:188
  23.4 5.0 %mixer_inside.1.y_ref = f32[768,512]{1,0:T(8,128)} custom-call(bf16[768,512]{1,0:T(8,128)(2,1)} %get-tuple-element.20.scaled_ref, bf16[768,64]{1,0:T(8,128)(2,1)} %get-tuple-element.21.write_ref, bf16[768,64]{1,0:T(8,128)(2,1)} %get-tuple-element.22.read_ref, f32[384,512]{1,0:T(8,128)} %get-tuple-element.23.before_ref, f32[8,768]{1,0:T(8,128)} %get-tuple-element.24.cum_ref), custom_call_target="tpu_custom_call" | custom-call | tf_op jit(solution)/shard_map/mixer_inside/pallas_call | solution.py:264
  29.3 4.9 %all-to-all-start = ((bf16[4,80,512]{2,1,0:T(8,128)(2,1)}), bf16[4,80,512]{2,1,0:T(8,128)(2,1)S(1)}, u32[]{:S(2)}, u32[]{:S(2)}) async-start(bf16[4,80,512]{2,1,0:T(8,128)(2,1)} %broadcast_in_dim.52), calls=%async_computation | async-start | bytes 655360 | tf_op jit(solution)/shard_map/all_to_all | solution.py:62
  34.2 6.3 %all-to-all-done = bf16[4,80,512]{2,1,0:T(8,128)(2,1)S(1)} async-done(((bf16[4,80,512]{2,1,0:T(8,128)(2,1)}), bf16[4,80,512]{2,1,0:T(8,128)(2,1)S(1)}, u32[]{:S(2)}, u32[]{:S(2)}) %all-to-all-start) | async-done | bytes 327712 | tf_op jit(solution)/shard_map/all_to_all | solution.py:62
  41.5 6.7 %all-to-all-start.1 = ((bf16[4,80,512]{2,1,0:T(8,128)(2,1)}), bf16[4,80,512]{2,1,0:T(8,128)(2,1)S(1)}, u32[]{:S(2)}, u32[]{:S(2)}) async-start(bf16[4,80,512]{2,1,0:T(8,128)(2,1)} %broadcast_in_dim.54), calls=%async_computation.1 | async-start | bytes 655360 | tf_op jit(solution)/shard_map/all_to_all | solution.py:62
  49.0 1.5 collective-permute-start.16
  51.7 2.5 %all-to-all-done.1 = bf16[4,80,512]{2,1,0:T(8,128)(2,1)S(1)} async-done(((bf16[4,80,512]{2,1,0:T(8,128)(2,1)}), bf16[4,80,512]{2,1,0:T(8,128)(2,1)S(1)}, u32[]{:S(2)}, u32[]{:S(2)}) %all-to-all-start.1) | async-done | bytes 327712 | tf_op jit(solution)/shard_map/all_to_all | solution.py:62
  55.1 3.7 %mixer_finish.1 = (bf16[384,512]{1,0:T(8,128)(2,1)}, bf16[384,512]{1,0:T(8,128)(2,1)}) custom-call(f32[768,512]{1,0:T(8,128)} %mixer_inside.1.y_ref, bf16[768,64]{1,0:T(8,128)(2,1)} %get-tuple-element.22.read_ref, f32[8,768]{1,0:T(8,128)} %get-tuple-element.25.grow_ref, bf16[768,512]{1,0:T(8,128)(2,1)} %gate_ref.1, f32[64,512]{1,0:T(8,128)} %fusion.3.state_ref, ...), custom_call_target="tpu_custom_call" | custom-call | tf_op jit(solution)/shard_map/mixer_finish/pallas_call | solution.py:302
  59.5 6.8 %collective-permute-start.8 = (bf16[16,512]{1,0:T(8,128)(2,1)S(1)}, bf16[16,512]{1,0:T(8,128)(2,1)S(1)}, u32[]{:S(2)}, u32[]{:S(2)}) collective-permute-start(bf16[16,512]{1,0:T(8,128)(2,1)S(1)} %slice.163), channel_id=1, source_target_pairs={{0,4},{4,8},{8,12},{12,16},{16,20},{20,24},{24,28},{28,32},{32,36}... | collective-permute-start | bytes 49160 | tf_op jit(solution)/shard_map/ppermute | solution.py:28
  69.9 2.6 %collective-permute-start.7 = (bf16[384,512]{1,0:T(8,128)(2,1)S(1)}, bf16[384,512]{1,0:T(8,128)(2,1)S(1)}, u32[]{:S(2)}, u32[]{:S(2)}) collective-permute-start(bf16[384,512]{1,0:T(8,128)(2,1)S(1)} %copy-done.15), channel_id=1, source_target_pairs={{0,3},{1,0},{2,1},{3,2},{4,7},{5,4},{6,5},{7,6},{8,11},{9,8},{10,9... | collective-permute-start | bytes 1179656 | tf_op jit(solution)/shard_map/ppermute | solution.py:28
  72.5 16.8 %collective-permute-done.2.p1 = bf16[384,512]{1,0:T(8,128)(2,1)S(1)} collective-permute-done((bf16[384,512]{1,0:T(8,128)(2,1)}, bf16[384,512]{1,0:T(8,128)(2,1)S(1)}, u32[]{:S(2)}, u32[]{:S(2)}) %collective-permute-start.2) | collective-permute-done | bytes 393248 | tf_op jit(solution)/shard_map/ppermute | solution.py:28
  92.7 8.2 %collective-permute-done.18 = bf16[64,4224]{1,0:T(8,128)(2,1)S(1)} collective-permute-done((bf16[64,4224]{1,0:T(8,128)(2,1)}, bf16[64,4224]{1,0:T(8,128)(2,1)S(1)}, u32[]{:S(2)}, u32[]{:S(2)}) %collective-permute-start.18) | collective-permute-done | bytes 540704 | tf_op jit(solution)/shard_map/ppermute | solution.py:43
  101.1 3.4 %collective-permute-done.3.p3a = bf16[384,512]{1,0:T(8,128)(2,1)S(1)} collective-permute-done((bf16[384,512]{1,0:T(8,128)(2,1)S(1)}, bf16[384,512]{1,0:T(8,128)(2,1)S(1)}, u32[]{:S(2)}, u32[]{:S(2)}) %collective-permute-start.3) | collective-permute-done | bytes 393248 | tf_op jit(solution)/shard_map/ppermute | solution.py:28
  104.4 2.7 %collective-permute-start.22 = (bf16[128,4224]{1,0:T(8,128)(2,1)S(1)}, bf16[128,4224]{1,0:T(8,128)(2,1)}, u32[]{:S(2)}, u32[]{:S(2)}) collective-permute-start(bf16[128,4224]{1,0:T(8,128)(2,1)S(1)} %constant_dynamic-update-slice_fusion.12), channel_id=1, source_target_pairs={{0,96},{4,28},{8,104},{12,4},{16,112},{20,12},{24,120},{28,20},{32... | collective-permute-start | bytes 3244040 | tf_op jit(solution)/shard_map/ppermute | solution.py:43
  107.1 3.7 %collective-permute-done.5.p3b = bf16[384,512]{1,0:T(8,128)(2,1)S(1)} collective-permute-done((bf16[384,512]{1,0:T(8,128)(2,1)S(1)}, bf16[384,512]{1,0:T(8,128)(2,1)S(1)}, u32[]{:S(2)}, u32[]{:S(2)}) %collective-permute-start.5) | collective-permute-done | bytes 393248 | tf_op jit(solution)/shard_map/ppermute | solution.py:28
  110.9 1.7 collective-permute-start.12
  112.7 22.4 %collective-permute-done.11.of = bf16[256,2048]{1,0:T(8,128)(2,1)S(1)} collective-permute-done((bf16[256,2048]{1,0:T(8,128)(2,1)S(1)}, bf16[256,2048]{1,0:T(8,128)(2,1)S(1)}, u32[]{:S(2)}, u32[]{:S(2)}) %collective-permute-start.11) | collective-permute-done | bytes 1048608 | tf_op jit(solution)/shard_map/ppermute | solution.py:28
  135.1 2.5 %collective-permute-start.26 = (bf16[2,2,32,4224]{3,2,1,0:T(8,128)(2,1)S(1)}, bf16[2,2,32,4224]{3,2,1,0:T(8,128)(2,1)S(1)}, u32[]{:S(2)}, u32[]{:S(2)}) collective-permute-start(bf16[2,2,32,4224]{3,2,1,0:T(8,128)(2,1)S(1)} %bitcast.91), channel_id=1, source_target_pairs={{0,4},{4,0},{1,5},{5,1},{2,6},{6,2},{3,7},{7,3},{8,12},{12,8},{9,1... | collective-permute-start | bytes 3244040 | tf_op jit(solution)/shard_map/ppermute | solution.py:32
  139.7 2.5 %collective-permute-start.24 = (bf16[128,4224]{1,0:T(8,128)(2,1)}, bf16[128,4224]{1,0:T(8,128)(2,1)}, u32[]{:S(2)}, u32[]{:S(2)}) collective-permute-start(bf16[128,4224]{1,0:T(8,128)(2,1)} %collective-permute-done.22), channel_id=1, source_target_pairs={{0,96},{4,28},{8,104},{12,4},{16,112},{20,12},{24,120},{28,20},{32... | collective-permute-start | bytes 3244040 | tf_op jit(solution)/shard_map/ppermute | solution.py:43
  142.7 10.5 %collective-permute-done.23 = bf16[128,4224]{1,0:T(8,128)(2,1)} collective-permute-done((bf16[128,4224]{1,0:T(8,128)(2,1)S(1)}, bf16[128,4224]{1,0:T(8,128)(2,1)}, u32[]{:S(2)}, u32[]{:S(2)}) %collective-permute-start.23) | collective-permute-done | bytes 1081376 | tf_op jit(solution)/shard_map/ppermute | solution.py:43
  156.4 3.3 %all-to-all-start.2 = ((bf16[4,16,512]{2,1,0:T(8,128)(2,1)}), bf16[4,16,512]{2,1,0:T(8,128)(2,1)S(1)}, u32[]{:S(2)}, u32[]{:S(2)}) async-start(bf16[4,16,512]{2,1,0:T(8,128)(2,1)} %broadcast_in_dim.58), calls=%async_computation.2 | async-start | bytes 131072 | tf_op jit(solution)/shard_map/all_to_all | solution.py:62
  160.3 3.8 %all-to-all-done.2.halo = bf16[4,16,512]{2,1,0:T(8,128)(2,1)S(1)} async-done(((bf16[4,16,512]{2,1,0:T(8,128)(2,1)}), bf16[4,16,512]{2,1,0:T(8,128)(2,1)S(1)}, u32[]{:S(2)}, u32[]{:S(2)}) %all-to-all-start.2) | async-done | bytes 65568 | tf_op jit(solution)/shard_map/all_to_all | solution.py:62
  164.7 13.3 %out_near.1.total_in = f32[784,2048]{1,0:T(8,128)} custom-call(s32[4]{0:T(128)} %pad_add_fusion.place_ref, bf16[384,512]{1,0:T(8,128)(2,1)} %get-tuple-element.27.p0, bf16[384,512]{1,0:T(8,128)(2,1)} %get-tuple-element.28.l0, bf16[384,512]{1,0:T(8,128)(2,1)} %copy-done.18, bf16[384,512]{1,0:T(8,128)(2,1)} %copy-done.17, bf16[384,512]{1,0:T(8,128)(2,1)} %copy-done.19, ...), custom_call_target="tpu_custom_call" | custom-call | tf_op jit(solution)/shard_map/out_near/pallas_call | solution.py:451
  178.1 30.9 %ffn.1 = (bf16[192,2048]{1,0:T(8,128)(2,1)}, bf16[192,2048]{1,0:T(8,128)(2,1)}, bf16[192,2048]{1,0:T(8,128)(2,1)}, bf16[96,2048]{1,0:T(8,128)(2,1)}, bf16[96,204...) custom-call(s32[4]{0:T(128)} %pad_add_fusion.place_ref, bf16[384,512]{1,0:T(8,128)(2,1)} %copy-done.20, ...), custom_call_target="tpu_custom_call" | custom-call | tf_op jit(solution)/shard_map/ffn/pallas_call | solution.py:617
  209.3 2.4 collective-permute-start.35
  211.7 8.2 %collective-permute-done.33 = bf16[96,2048]{1,0:T(8,128)(2,1)S(1)} collective-permute-done((bf16[96,2048]{1,0:T(8,128)(2,1)}, bf16[96,2048]{1,0:T(8,128)(2,1)S(1)}, u32[]{:S(2)}, u32[]{:S(2)}) %collective-permute-start.33) | collective-permute-done | bytes 393248 | tf_op jit(solution)/shard_map/ppermute | solution.py:28
  221.5 2.7 %collective-permute-start.36 = (bf16[192,2048]{1,0:T(8,128)(2,1)S(1)}, bf16[192,2048]{1,0:T(8,128)(2,1)S(1)}, u32[]{:S(2)}, u32[]{:S(2)}) collective-permute-start(bf16[192,2048]{1,0:T(8,128)(2,1)S(1)} %add_convert_fusion.1), channel_id=1, source_target_pairs={{0,3},{1,0},{2,1},{3,2},{4,7},{5,4},{6,5},{7,6},{8,11},{9,8},{10,9... | collective-permute-start | bytes 2359304 | tf_op jit(solution)/shard_map/ppermute | solution.py:28
  224.2 15.4 %collective-permute-done.34 = bf16[192,2048]{1,0:T(8,128)(2,1)S(1)} collective-permute-done((bf16[192,2048]{1,0:T(8,128)(2,1)S(1)}, bf16[192,2048]{1,0:T(8,128)(2,1)S(1)}, u32[]{:S(2)}, u32[]{:S(2)}) %collective-permute-start.34) | collective-permute-done | bytes 786464 | tf_op jit(solution)/shard_map/ppermute | solution.py:28
  239.5 1.4 add_convert_fusion
  (161 shorter events, 28.1 us)
Async XLA Ops:
  2.4 67.5 %collective-permute-start.9 = (bf16[256,2048]{1,0:T(8,128)(2,1)}, bf16[256,2048]{1,0:T(8,128)(2,1)S(1)}, u32[]{:S(2)}, u32[]{:S(2)}) collective-permute-start(bf16[256,2048]{1,0:T(8,128)(2,1)} %constant_dynamic-slice_fusion), channel_id=1, source_target_pairs={{0,1},{1,2},{2,3},{3,0},{4,5},{5,6},{6,7},{7,4},{8,9},{9,10},{10,1... | collective-permute-start | bytes 3145736 | tf_op jit(solution)/shard_map/ppermute | solution.py:28
  4.4 68.1 %collective-permute-start.10 = (bf16[256,2048]{1,0:T(8,128)(2,1)}, bf16[256,2048]{1,0:T(8,128)(2,1)}, u32[]{:S(2)}, u32[]{:S(2)}) collective-permute-start(bf16[256,2048]{1,0:T(8,128)(2,1)} %constant_dynamic-slice_fusion), channel_id=1, source_target_pairs={{0,3},{1,0},{2,1},{3,2},{4,7},{5,4},{6,5},{7,6},{8,11},{9,8},{10,9... | collective-permute-start | bytes 3145736 | tf_op jit(solution)/shard_map/ppermute | solution.py:28
  22.0 12.2 %collective-permute-start.15 = (bf16[32,4224]{1,0:T(8,128)(2,1)S(1)}, bf16[32,4224]{1,0:T(8,128)(2,1)S(1)}, u32[]{:S(2)}, u32[]{:S(2)}) collective-permute-start(bf16[32,4224]{1,0:T(8,128)(2,1)S(1)} %broadcast_select_fusion.2), channel_id=1, source_target_pairs={{0,4},{4,0},{1,5},{5,1},{2,6},{6,2},{3,7},{7,3},{8,12},{12,8},{9,1... | collective-permute-start | bytes 811016 | tf_op jit(solution)/shard_map/ppermute | solution.py:32
  29.3 11.3 %all-to-all-start = ((bf16[4,80,512]{2,1,0:T(8,128)(2,1)}), bf16[4,80,512]{2,1,0:T(8,128)(2,1)S(1)}, u32[]{:S(2)}, u32[]{:S(2)}) async-start(bf16[4,80,512]{2,1,0:T(8,128)(2,1)} %broadcast_in_dim.52), calls=%async_computation | async-start | bytes 655360 | tf_op jit(solution)/shard_map/all_to_all | solution.py:62
  41.5 12.6 %all-to-all-start.1 = ((bf16[4,80,512]{2,1,0:T(8,128)(2,1)}), bf16[4,80,512]{2,1,0:T(8,128)(2,1)S(1)}, u32[]{:S(2)}, u32[]{:S(2)}) async-start(bf16[4,80,512]{2,1,0:T(8,128)(2,1)} %broadcast_in_dim.54), calls=%async_computation.1 | async-start | bytes 655360 | tf_op jit(solution)/shard_map/all_to_all | solution.py:62
  49.0 19.4 %collective-permute-start.16 = (bf16[64,4224]{1,0:T(8,128)(2,1)}, bf16[64,4224]{1,0:T(8,128)(2,1)}, u32[]{:S(2)}, u32[]{:S(2)}) collective-permute-start(bf16[64,4224]{1,0:T(8,128)(2,1)} %pad_maximum_fusion.1), channel_id=1, source_target_pairs={{0,8},{4,36},{8,16},{12,44},{16,24},{20,52},{24,0},{28,60},{32,40}... | collective-permute-start | bytes 1622024 | tf_op jit(solution)/shard_map/ppermute | solution.py:43
  50.5 18.1 %collective-permute-start.17 = (bf16[64,4224]{1,0:T(8,128)(2,1)}, bf16[64,4224]{1,0:T(8,128)(2,1)}, u32[]{:S(2)}, u32[]{:S(2)}) collective-permute-start(bf16[64,4224]{1,0:T(8,128)(2,1)} %pad_maximum_fusion.1), channel_id=1, source_target_pairs={{0,24},{4,100},{8,0},{12,108},{16,8},{20,116},{24,16},{28,124},{32... | collective-permute-start | bytes 1622024 | tf_op jit(solution)/shard_map/ppermute | solution.py:43
  67.1 23.3 %collective-permute-start.4 = (bf16[384,512]{1,0:T(8,128)(2,1)}, bf16[384,512]{1,0:T(8,128)(2,1)S(1)}, u32[]{:S(2)}, u32[]{:S(2)}) collective-permute-start(bf16[384,512]{1,0:T(8,128)(2,1)} %get-tuple-element.28.l0), channel_id=1, source_target_pairs={{0,3},{1,0},{2,1},{3,2},{4,7},{5,4},{6,5},{7,6},{8,11},{9,8},{10,9... | collective-permute-start | bytes 1179656 | tf_op jit(solution)/shard_map/ppermute | solution.py:28
  68.4 22.6 %collective-permute-start.6 = (bf16[384,512]{1,0:T(8,128)(2,1)}, bf16[384,512]{1,0:T(8,128)(2,1)S(1)}, u32[]{:S(2)}, u32[]{:S(2)}) collective-permute-start(bf16[384,512]{1,0:T(8,128)(2,1)} %get-tuple-element.28.l0), channel_id=1, source_target_pairs={{0,1},{1,2},{2,3},{3,0},{4,5},{5,6},{6,7},{7,4},{8,9},{9,10},{10,1... | collective-permute-start | bytes 1179656 | tf_op jit(solution)/shard_map/ppermute | solution.py:28
  68.6 20.7 %collective-permute-start.2 = (bf16[384,512]{1,0:T(8,128)(2,1)}, bf16[384,512]{1,0:T(8,128)(2,1)S(1)}, u32[]{:S(2)}, u32[]{:S(2)}) collective-permute-start(bf16[384,512]{1,0:T(8,128)(2,1)} %get-tuple-element.27.p0), channel_id=1, source_target_pairs={{0,1},{1,2},{2,3},{3,0},{4,5},{5,6},{6,7},{7,4},{8,9},{9,10},{10,1... | collective-permute-start | bytes 1179656 | tf_op jit(solution)/shard_map/ppermute | solution.py:28
  69.9 22.7 %collective-permute-start.7 = (bf16[384,512]{1,0:T(8,128)(2,1)S(1)}, bf16[384,512]{1,0:T(8,128)(2,1)S(1)}, u32[]{:S(2)}, u32[]{:S(2)}) collective-permute-start(bf16[384,512]{1,0:T(8,128)(2,1)S(1)} %copy-done.15), channel_id=1, source_target_pairs={{0,3},{1,0},{2,1},{3,2},{4,7},{5,4},{6,5},{7,6},{8,11},{9,8},{10,9... | collective-permute-start | bytes 1179656 | tf_op jit(solution)/shard_map/ppermute | solution.py:28
  72.5 38.3 %collective-permute-start.19 = (bf16[128,4224]{1,0:T(8,128)(2,1)S(1)}, bf16[128,4224]{1,0:T(8,128)(2,1)S(1)}, u32[]{:S(2)}, u32[]{:S(2)}) collective-permute-start(bf16[128,4224]{1,0:T(8,128)(2,1)S(1)} %pad_maximum_fusion), channel_id=1, source_target_pairs={{0,32},{4,12},{8,40},{12,20},{16,48},{20,28},{24,56},{28,4},{32,64... | collective-permute-start | bytes 3244040 | tf_op jit(solution)/shard_map/ppermute | solution.py:43
  89.3 23.3 %collective-permute-start.21 = (bf16[128,4224]{1,0:T(8,128)(2,1)S(1)}, bf16[128,4224]{1,0:T(8,128)(2,1)}, u32[]{:S(2)}, u32[]{:S(2)}) collective-permute-start(bf16[128,4224]{1,0:T(8,128)(2,1)S(1)} %pad_maximum_fusion), channel_id=1, source_target_pairs={{0,96},{4,28},{8,104},{12,4},{16,112},{20,12},{24,120},{28,20},{32... | collective-permute-start | bytes 3244040 | tf_op jit(solution)/shard_map/ppermute | solution.py:43
  90.4 22.3 %collective-permute-start.25 = (bf16[2,2,32,4224]{3,2,1,0:T(8,128)(2,1)S(1)}, bf16[2,2,32,4224]{3,2,1,0:T(8,128)(2,1)S(1)}, u32[]{:S(2)}, u32[]{:S(2)}) collective-permute-start(bf16[2,2,32,4224]{3,2,1,0:T(8,128)(2,1)S(1)} %bitcast.89), channel_id=1, source_target_pairs={{0,4},{4,0},{1,5},{5,1},{2,6},{6,2},{3,7},{7,3},{8,12},{12,8},{9,1... | collective-permute-start | bytes 3244040 | tf_op jit(solution)/shard_map/ppermute | solution.py:32
  92.6 11.8 %collective-permute-start.3 = (bf16[384,512]{1,0:T(8,128)(2,1)S(1)}, bf16[384,512]{1,0:T(8,128)(2,1)S(1)}, u32[]{:S(2)}, u32[]{:S(2)}) collective-permute-start(bf16[384,512]{1,0:T(8,128)(2,1)S(1)} %collective-permute-done.2.p1), channel_id=1, source_target_pairs={{0,1},{1,2},{2,3},{3,0},{4,5},{5,6},{6,7},{7,4},{8,9},{9,10},{10,1... | collective-permute-start | bytes 1179656 | tf_op jit(solution)/shard_map/ppermute | solution.py:28
  104.4 35.3 %collective-permute-start.22 = (bf16[128,4224]{1,0:T(8,128)(2,1)S(1)}, bf16[128,4224]{1,0:T(8,128)(2,1)}, u32[]{:S(2)}, u32[]{:S(2)}) collective-permute-start(bf16[128,4224]{1,0:T(8,128)(2,1)S(1)} %constant_dynamic-update-slice_fusion.12), channel_id=1, source_target_pairs={{0,96},{4,28},{8,104},{12,4},{16,112},{20,12},{24,120},{28,20},{32... | collective-permute-start | bytes 3244040 | tf_op jit(solution)/shard_map/ppermute | solution.py:43
  110.9 24.3 %collective-permute-start.11 = (bf16[256,2048]{1,0:T(8,128)(2,1)S(1)}, bf16[256,2048]{1,0:T(8,128)(2,1)S(1)}, u32[]{:S(2)}, u32[]{:S(2)}) collective-permute-start(bf16[256,2048]{1,0:T(8,128)(2,1)S(1)} %copy-done.9), channel_id=1, source_target_pairs={{0,1},{1,2},{2,3},{3,0},{4,5},{5,6},{6,7},{7,4},{8,9},{9,10},{10,1... | collective-permute-start | bytes 3145736 | tf_op jit(solution)/shard_map/ppermute | solution.py:28
  110.9 26.8 %collective-permute-start.12 = (bf16[256,2048]{1,0:T(8,128)(2,1)S(1)}, bf16[256,2048]{1,0:T(8,128)(2,1)S(1)}, u32[]{:S(2)}, u32[]{:S(2)}) collective-permute-start(bf16[256,2048]{1,0:T(8,128)(2,1)S(1)} %copy-done.9), channel_id=1, source_target_pairs={{0,4},{4,0},{1,5},{5,1},{2,6},{6,2},{3,7},{7,3},{8,12},{12,8},{9,1... | collective-permute-start | bytes 3145736 | tf_op jit(solution)/shard_map/ppermute | solution.py:32
  112.6 25.8 %collective-permute-start.13 = (bf16[256,2048]{1,0:T(8,128)(2,1)}, bf16[256,2048]{1,0:T(8,128)(2,1)S(1)}, u32[]{:S(2)}, u32[]{:S(2)}) collective-permute-start(bf16[256,2048]{1,0:T(8,128)(2,1)} %collective-permute-done.10.oa), channel_id=1, source_target_pairs={{0,4},{4,0},{1,5},{5,1},{2,6},{6,2},{3,7},{7,3},{8,12},{12,8},{9,1... | collective-permute-start | bytes 3145736 | tf_op jit(solution)/shard_map/ppermute | solution.py:32
  112.7 29.5 %collective-permute-start.20 = (bf16[128,4224]{1,0:T(8,128)(2,1)S(1)}, bf16[128,4224]{1,0:T(8,128)(2,1)}, u32[]{:S(2)}, u32[]{:S(2)}) collective-permute-start(bf16[128,4224]{1,0:T(8,128)(2,1)S(1)} %constant_dynamic-update-slice_fusion.12), channel_id=1, source_target_pairs={{0,32},{4,12},{8,40},{12,20},{16,48},{20,28},{24,56},{28,4},{32,64... | collective-permute-start | bytes 3244040 | tf_op jit(solution)/shard_map/ppermute | solution.py:43
  137.6 15.6 %collective-permute-start.23 = (bf16[128,4224]{1,0:T(8,128)(2,1)S(1)}, bf16[128,4224]{1,0:T(8,128)(2,1)}, u32[]{:S(2)}, u32[]{:S(2)}) collective-permute-start(bf16[128,4224]{1,0:T(8,128)(2,1)S(1)} %collective-permute-done.19), channel_id=1, source_target_pairs={{0,32},{4,12},{8,40},{12,20},{16,48},{20,28},{24,56},{28,4},{32,64... | collective-permute-start | bytes 3244040 | tf_op jit(solution)/shard_map/ppermute | solution.py:43
  139.7 14.5 %collective-permute-start.27 = (bf16[2,2,32,4224]{3,2,1,0:T(8,128)(2,1)S(1)}, bf16[2,2,32,4224]{3,2,1,0:T(8,128)(2,1)S(1)}, u32[]{:S(2)}, u32[]{:S(2)}) collective-permute-start(bf16[2,2,32,4224]{3,2,1,0:T(8,128)(2,1)S(1)} %bitcast.93), channel_id=1, source_target_pairs={{0,4},{4,0},{1,5},{5,1},{2,6},{6,2},{3,7},{7,3},{8,12},{12,8},{9,1... | collective-permute-start | bytes 3244040 | tf_op jit(solution)/shard_map/ppermute | solution.py:32
  139.7 15.1 %collective-permute-start.24 = (bf16[128,4224]{1,0:T(8,128)(2,1)}, bf16[128,4224]{1,0:T(8,128)(2,1)}, u32[]{:S(2)}, u32[]{:S(2)}) collective-permute-start(bf16[128,4224]{1,0:T(8,128)(2,1)} %collective-permute-done.22), channel_id=1, source_target_pairs={{0,96},{4,28},{8,104},{12,4},{16,112},{20,12},{24,120},{28,20},{32... | collective-permute-start | bytes 3244040 | tf_op jit(solution)/shard_map/ppermute | solution.py:43
  142.2 12.1 %collective-permute-start.14 = (bf16[256,2048]{1,0:T(8,128)(2,1)S(1)}, bf16[256,2048]{1,0:T(8,128)(2,1)S(1)}, u32[]{:S(2)}, u32[]{:S(2)}) collective-permute-start(bf16[256,2048]{1,0:T(8,128)(2,1)S(1)} %collective-permute-done.11.of), channel_id=1, source_target_pairs={{0,4},{4,0},{1,5},{5,1},{2,6},{6,2},{3,7},{7,3},{8,12},{12,8},{9,1... | collective-permute-start | bytes 3145736 | tf_op jit(solution)/shard_map/ppermute | solution.py:32
  142.2 35.8 %collective-permute-start.29 = (bf16[2,2,32,4224]{3,2,1,0:T(8,128)(2,1)}, bf16[2,2,32,4224]{3,2,1,0:T(8,128)(2,1)}, u32[]{:S(2)}, u32[]{:S(2)}) collective-permute-start(bf16[2,2,32,4224]{3,2,1,0:T(8,128)(2,1)} %bitcast.37.w4), channel_id=1, source_target_pairs={{0,4},{4,0},{1,5},{5,1},{2,6},{6,2},{3,7},{7,3},{8,12},{12,8},{9,1... | collective-permute-start | bytes 3244040 | tf_op jit(solution)/shard_map/ppermute | solution.py:32
  153.3 24.8 %collective-permute-start.30 = (bf16[2,2,32,4224]{3,2,1,0:T(8,128)(2,1)}, bf16[2,2,32,4224]{3,2,1,0:T(8,128)(2,1)}, u32[]{:S(2)}, u32[]{:S(2)}) collective-permute-start(bf16[2,2,32,4224]{3,2,1,0:T(8,128)(2,1)} %bitcast.38.w5), channel_id=1, source_target_pairs={{0,4},{4,0},{1,5},{5,1},{2,6},{6,2},{3,7},{7,3},{8,12},{12,8},{9,1... | collective-permute-start | bytes 3244040 | tf_op jit(solution)/shard_map/ppermute | solution.py:32
  154.2 23.8 %collective-permute-start.28 = (bf16[2,2,32,4224]{3,2,1,0:T(8,128)(2,1)}, bf16[2,2,32,4224]{3,2,1,0:T(8,128)(2,1)}, u32[]{:S(2)}, u32[]{:S(2)}) collective-permute-start(bf16[2,2,32,4224]{3,2,1,0:T(8,128)(2,1)} %bitcast.36.w3), channel_id=1, source_target_pairs={{0,4},{4,0},{1,5},{5,1},{2,6},{6,2},{3,7},{7,3},{8,12},{12,8},{9,1... | collective-permute-start | bytes 3244040 | tf_op jit(solution)/shard_map/ppermute | solution.py:32
  154.3 23.8 %collective-permute-start.31 = (bf16[2,2,32,4224]{3,2,1,0:T(8,128)(2,1)}, bf16[2,2,32,4224]{3,2,1,0:T(8,128)(2,1)}, u32[]{:S(2)}, u32[]{:S(2)}) collective-permute-start(bf16[2,2,32,4224]{3,2,1,0:T(8,128)(2,1)} %bitcast.39.w6), channel_id=1, source_target_pairs={{0,4},{4,0},{1,5},{5,1},{2,6},{6,2},{3,7},{7,3},{8,12},{12,8},{9,1... | collective-permute-start | bytes 3244040 | tf_op jit(solution)/shard_map/ppermute | solution.py:32
  155.2 22.9 %collective-permute-start.32 = (bf16[2,2,32,4224]{3,2,1,0:T(8,128)(2,1)}, bf16[2,2,32,4224]{3,2,1,0:T(8,128)(2,1)}, u32[]{:S(2)}, u32[]{:S(2)}) collective-permute-start(bf16[2,2,32,4224]{3,2,1,0:T(8,128)(2,1)} %bitcast.40.w7), channel_id=1, source_target_pairs={{0,4},{4,0},{1,5},{5,1},{2,6},{6,2},{3,7},{7,3},{8,12},{12,8},{9,1... | collective-permute-start | bytes 3244040 | tf_op jit(solution)/shard_map/ppermute | solution.py:32
  209.3 12.0 %collective-permute-start.35 = (bf16[96,2048]{1,0:T(8,128)(2,1)}, bf16[96,2048]{1,0:T(8,128)(2,1)S(1)}, u32[]{:S(2)}, u32[]{:S(2)}) collective-permute-start(bf16[96,2048]{1,0:T(8,128)(2,1)} %get-tuple-element.34), channel_id=1, source_target_pairs={{0,3},{1,0},{2,1},{3,2},{4,7},{5,4},{6,5},{7,6},{8,11},{9,8},{10,9... | collective-permute-start | bytes 1179656 | tf_op jit(solution)/shard_map/ppermute | solution.py:28
  221.2 18.3 %collective-permute-start.34 = (bf16[192,2048]{1,0:T(8,128)(2,1)S(1)}, bf16[192,2048]{1,0:T(8,128)(2,1)S(1)}, u32[]{:S(2)}, u32[]{:S(2)}) collective-permute-start(bf16[192,2048]{1,0:T(8,128)(2,1)S(1)} %add_convert_fusion.2), channel_id=1, source_target_pairs={{0,1},{1,2},{2,3},{3,0},{4,5},{5,6},{6,7},{7,4},{8,9},{9,10},{10,1... | collective-permute-start | bytes 2359304 | tf_op jit(solution)/shard_map/ppermute | solution.py:28
  221.5 18.1 %collective-permute-start.36 = (bf16[192,2048]{1,0:T(8,128)(2,1)S(1)}, bf16[192,2048]{1,0:T(8,128)(2,1)S(1)}, u32[]{:S(2)}, u32[]{:S(2)}) collective-permute-start(bf16[192,2048]{1,0:T(8,128)(2,1)S(1)} %add_convert_fusion.1), channel_id=1, source_target_pairs={{0,3},{1,0},{2,1},{3,2},{4,7},{5,4},{6,5},{7,6},{8,11},{9,8},{10,9... | collective-permute-start | bytes 2359304 | tf_op jit(solution)/shard_map/ppermute | solution.py:28
  (37 other events, 650.4 us)
